TPU v7x, 32 devices: a whole 2x2x4 slice. The times are simulated.
32 devices in a mesh: sp: 16 (over z, y, x), tp: 2 (over core).
Axes of the slice: x: 2, y: 2, z: 4, core: 2. Of those that a mesh axis runs over, the one named last changes fastest.
Arguments:
- queries: bfloat16 [4096, 1024], P('sp', 'tp'), may hold values from -6 to 6
- keys: bfloat16 [4096, 512], P('sp', 'tp'), may hold values from -6 to 6
- values: bfloat16 [4096, 512], P('sp', 'tp'), may hold values from -6 to 6
- q_gain: float32 [64], replicated, may hold values from 1.6 to 4.5
- key_norm_gain: float32 [64], replicated, may hold values from 1.6 to 4.5
- out_weight: bfloat16 [1024, 2048], P('tp'), may hold values from -0.1875 to 0.1875
- residual: bfloat16 [4096, 2048], P('sp'), may hold values from -6 to 6
- ln1_gain: float32 [2048], replicated, may hold values from 0.1 to 1.9
- ln1_bias: float32 [2048], replicated, may hold values from -3 to 3
- up_weight: bfloat16 [2048, 8192], P('sp', 'tp'), may hold values from -0.125 to 0.125
- down_weight: bfloat16 [8192, 2048], P('tp', 'sp'), may hold values from -0.0625 to 0.0625
- ln2_gain: float32 [2048], replicated, may hold values from 0.1 to 1.9
- ln2_bias: float32 [2048], replicated, may hold values from -3 to 3
Outputs:
- encoded: bfloat16 [4096, 2048], P('sp', 'tp')
All inputs are finite; a program needn't handle non-finite values.
Results may differ from a plain program's by a relative error of at most 0.014.
Values may be sent and summed in bfloat16 or wider, within the bound.
No kernel may reach another device: no remote copies, remote signals or barrier semaphores. Data moves between devices by JAX's collectives and lax.ppermute only.
A program may use at most 128 MiB of HBM per device.

v0:
```python
import math

import jax
import jax.numpy as jnp
from jax import lax
from jax.sharding import PartitionSpec as P

D = 2048
HEAD_SIZE = 64
GRID_W = 64


ALPHA = 8.0**0.25
ROTARY_BASE = 10000.0
RMS_EPSILON = 1e-06
NORM_EPSILON = 1e-05


def rotate_grid(heads_in, grid_places):
    half_dim = heads_in.shape[-1] // 2
    quarter = half_dim // 2
    inverse = ROTARY_BASE ** (-jnp.arange(quarter, dtype=jnp.float32) / quarter)

    def spin(segment, coords):
        angles = coords.astype(jnp.float32)[:, None] * inverse[None, :]
        cos_val = jnp.cos(angles)[:, None, :]
        sin_val = jnp.sin(angles)[:, None, :]
        lead_half = segment[..., :quarter]
        tail_half = segment[..., quarter:]
        return jnp.concatenate(
            [lead_half * cos_val - tail_half * sin_val, tail_half * cos_val + lead_half * sin_val],
            -1,
        )

    return jnp.concatenate(
        [
            spin(heads_in[..., :half_dim], grid_places // GRID_W),
            spin(heads_in[..., half_dim:], grid_places % GRID_W),
        ],
        -1,
    )


def prepare_inputs(heads_in, gain_vec, grid_places, factor):
    values32 = heads_in.astype(jnp.float32)
    normed = (
        values32
        * lax.rsqrt(jnp.mean(values32 * values32, -1, keepdims=True) + RMS_EPSILON)
        * gain_vec
    )
    return (rotate_grid(normed, grid_places) * factor).astype(jnp.bfloat16)


def layer_norm(pre_norm, gain_vec, bias_vec):
    row_mean = jnp.mean(pre_norm, -1, keepdims=True)
    centred = pre_norm - row_mean
    spread = jnp.mean(centred * centred, -1, keepdims=True)
    return centred * lax.rsqrt(spread + NORM_EPSILON) * gain_vec + bias_vec


def finish_norm(pre_norm, stats, gain_vec, bias_vec):
    row_mean = stats[0][:, None] / D
    spread = stats[1][:, None] / D - row_mean * row_mean
    return (pre_norm - row_mean) * lax.rsqrt(spread + NORM_EPSILON) * gain_vec + bias_vec


def take_cols(array_in, col_start, col_width):
    return lax.dynamic_slice_in_dim(array_in, col_start, col_width, array_in.ndim - 1)


def local(
    queries,
    keys,
    values,
    q_gain,
    key_norm_gain,
    out_weight,
    residual,
    ln1_gain,
    ln1_bias,
    up_weight,
    down_weight,
    ln2_gain,
    ln2_bias,
):
    tok_rows = queries.shape[0]
    grid_places = lax.axis_index("sp") * tok_rows + jnp.arange(tok_rows, dtype=jnp.int32)
    kv_heads = keys.shape[1] // HEAD_SIZE
    q_count = queries.shape[1] // HEAD_SIZE
    group_count_size = q_count // kv_heads
    query_head_rows = prepare_inputs(
        queries.reshape(tok_rows, q_count, HEAD_SIZE), q_gain, grid_places, HEAD_SIZE ** (-0.5)
    )
    q_grouped = query_head_rows.reshape(tok_rows, kv_heads, group_count_size, HEAD_SIZE)
    k_sent = prepare_inputs(
        keys.reshape(tok_rows, kv_heads, HEAD_SIZE), key_norm_gain, grid_places, 1.0
    ).reshape(tok_rows, kv_heads * HEAD_SIZE)
    initial = (
        jnp.full((kv_heads, group_count_size, tok_rows), -jnp.inf, jnp.float32),
        jnp.zeros((kv_heads, group_count_size, tok_rows), jnp.float32),
        jnp.zeros((tok_rows, kv_heads, group_count_size, HEAD_SIZE), jnp.float32),
    )
    key_piece = lax.all_gather(k_sent, "sp", axis=0, tiled=True)
    value_piece = lax.all_gather(values, "sp", axis=0, tiled=True)
    key_count = key_piece.shape[0]
    block_len = math.gcd(key_count, 2048)
    key_blocks = key_piece.reshape(key_count // block_len, block_len, kv_heads, HEAD_SIZE)
    value_blocks = value_piece.reshape(key_count // block_len, block_len, kv_heads, HEAD_SIZE)

    def advance(state_in, blocks):
        maxima, totals, accumulated = state_in
        scores = jnp.einsum(
            "qhgd,khd->hgqk", q_grouped, blocks[0], preferred_element_type=jnp.float32
        )
        new_max = jnp.maximum(maxima, jnp.max(scores, -1))
        factor = jnp.exp(maxima - new_max)
        weights = jnp.exp(scores - new_max[..., None])
        totals = totals * factor + jnp.sum(weights, -1)
        update = jnp.einsum(
            "hgqk,khd->qhgd",
            weights.astype(jnp.bfloat16),
            blocks[1],
            preferred_element_type=jnp.float32,
        )
        accumulated = accumulated * jnp.transpose(factor, (2, 0, 1))[..., None] + update
        return ((new_max, totals, accumulated), None)

    state_out, unused = lax.scan(advance, initial, (key_blocks, value_blocks))
    maxima, totals, accumulated = state_out
    attended = (
        (accumulated / jnp.transpose(totals, (2, 0, 1))[..., None])
        .reshape(tok_rows, q_count * HEAD_SIZE)
        .astype(jnp.bfloat16)
    )
    partial_value = jnp.dot(attended, out_weight, preferred_element_type=jnp.float32)
    col_width = D // lax.axis_size("tp")
    col_start = lax.axis_index("tp") * col_width
    mixed_sum = lax.psum(partial_value.astype(jnp.bfloat16), "tp").astype(jnp.float32)
    full_rows = layer_norm(
        ALPHA * residual.astype(jnp.float32) + mixed_sum, ln1_gain, ln1_bias
    ).astype(jnp.bfloat16)
    normed_own = take_cols(full_rows, col_start, col_width)
    up_acts = jnp.dot(
        full_rows,
        lax.all_gather(up_weight, "sp", axis=0, tiled=True),
        preferred_element_type=jnp.float32,
    )
    hidden = jnp.square(jnp.maximum(up_acts, 0.0)).astype(jnp.bfloat16)
    partial_ffn = jnp.dot(
        hidden,
        lax.all_gather(down_weight, "sp", axis=1, tiled=True),
        preferred_element_type=jnp.float32,
    )
    ffn_cols = lax.psum_scatter(
        partial_ffn.astype(jnp.bfloat16), "tp", scatter_dimension=1, tiled=True
    ).astype(jnp.float32)
    second = ALPHA * normed_own.astype(jnp.float32) + ffn_cols
    stats_two = lax.psum((jnp.sum(second, -1), jnp.sum(second * second, -1)), "tp")
    return finish_norm(
        second,
        stats_two,
        take_cols(ln2_gain, col_start, col_width),
        take_cols(ln2_bias, col_start, col_width),
    ).astype(jnp.bfloat16)


def solution(mesh):
    return jax.shard_map(
        local,
        mesh=mesh,
        in_specs=(
            P("sp", "tp"),
            P("sp", "tp"),
            P("sp", "tp"),
            P(),
            P(),
            P("tp", None),
            P("sp", None),
            P(),
            P(),
            P("sp", "tp"),
            P("tp", "sp"),
            P(),
            P(),
        ),
        out_specs=P("sp", "tp"),
        check_vma=False,
    )
```

profile of v0, /device:TPU:9, one launch (start us, length us, event | category | flops | bytes accessed | tf_op | source)
XLA Modules:
  0.0 703.6 jit_solution(7267192037591548552)
XLA Ops:
  6.5 0.0 copy-start
  6.5 0.0 all-gather.5.cloned.1.call-start
  6.6 1.1 copy.21
  7.8 0.7 fusion.30
  8.5 0.2 multiply_cosine_fusion.1
  8.8 0.7 pad_maximum_fusion
  9.4 0.0 all-gather.5.cloned.1.call-update
  9.5 0.0 all-gather.7.cloned.1.call-start
  9.5 0.7 all-gather.7.cloned.1.call-update
  10.2 0.0 all-reduce.3.cloned.1.call-start
  10.3 1.1 copy.22
  11.4 0.1 fusion.26
  11.5 0.1 fusion.27
  11.6 0.1 multiply_subtract_fusion.1
  11.7 60.6 %all-gather.5.cloned.1.call-done = bf16[4096,256]{0,1:T(8,128)(2,1)} async-done(((bf16[256,256]{0,1:T(8,128)(2,1)}), bf16[4096,256]{0,1:T(8,128)(2,1)}) %all-gather.5.cloned.1.call-update) | async-done | bytes 2097168 | tf_op jit(solution)/shard_map/all_gather | solution.py:103
  72.3 4.5 reshape.201
  76.8 3.8 copy.24
  80.6 56.0 %all-gather.7.cloned.1.call-done = bf16[4096,256]{1,0:T(8,128)(2,1)} async-done(((bf16[256,256]{1,0:T(8,128)(2,1)}), bf16[4096,256]{1,0:T(8,128)(2,1)}) %all-gather.7.cloned.1.call-update) | async-done | bytes 2097168 | tf_op jit(solution)/shard_map/all_gather | solution.py:104
  136.6 7.1 %reshape.207 = bf16[2,2048,4,64]{3,2,1,0:T(4,128)(2,1)} reshape(bf16[4096,256]{1,0:T(8,128)(2,1)} %all-gather.7.cloned.1.call-done) | data formatting | bytes 4194304 | tf_op jit(solution)/shard_map/reshape | solution.py:108
  143.6 6.9 copy.25
  150.6 49.9 %while.15 = (s32[]{:T(128)}, f32[4,2,256]{2,1,0:T(2,128)S(1)}, f32[4,2,256]{2,1,0:T(2,128)S(1)}, f32[256,4,2,64]{0,3,2,1:T(8,128)S(1)}, bf16[2,2048,4,64]{1,3,2,...) while((s32[]{:T(128)}, f32[4,2,256]{2,1,0:T(2,128)S(1)}, ...), condition=%wide.region_5.6_spmd.clone, body=%wide.region_2.5_spmd.clone.sunk | while | flops 1095118848 | bytes 53871716 | solution.py:128
  150.6 9.3 %bitcast_reduce_fusion.2 = (f32[4,2,256]{2,1,0:T(2,128)S(1)}, f32[4,2048,256,2]{2,1,3,0:T(8,128)}) fusion(bf16[256,4,2,64]{0,3,2,1:T(8,128)(2,1)S(1)} %get-tuple-element.194, bf16[2,2048,4,64]{1,3,2,0:T(8,128)(2,1)} %get-tuple-element.193, s32[]{:T(128)} %get-tuple-element.180), kind=kOutput, calls=%fused_computation.1.clone.1 | convolution fusion | flops 541063168 | bytes 18096640 | tf_op jit(solution)/shard_map/while/body/eval_jaxpr/qhgd,khd->hgqk/dot_general | solution.py:112
  159.9 7.6 %fusion.55 = f32[256,4,2,64]{0,3,2,1:T(8,128)S(1)} fusion(f32[4,2048,256,2]{2,1,3,0:T(8,128)} %get-tuple-element.169, f32[4,2,256]{2,1,0:T(2,128)S(1)} %get-tuple-element.190, bf16[2,2048,4,64]{1,3,2,0:T(8,128)(2,1)} %get-tuple-element.195, s32[]{:T(128)} %get-tuple-element.180, f32[256,4,2,64]{0,3,2,1:T(8,128)S(1)} %get-tuple-element.183, ...), kind=kOutput, calls=%fused_computation.8.clone.1 | convolution fusion | flops 545652736 | bytes 18891264 | tf_op jit(solution)/shard_map/while/body/eval_jaxpr/hgqk,khd->qhgd/dot_general | solution.py:119
  167.5 8.0 %fusion.53 = f32[4,2,256]{2,1,0:T(2,128)S(1)} fusion(f32[4,2048,256,2]{2,1,3,0:T(8,128)} %get-tuple-element.169, f32[4,2,256]{2,1,0:T(2,128)S(1)} %get-tuple-element.190), kind=kLoop, calls=%fused_computation.4.clone.1 | loop fusion | flops 8386560 | bytes 16793600 | tf_op jit(solution)/shard_map/while/body/eval_jaxpr/reduce_sum | solution.py:118
  175.6 9.3 %bitcast_reduce_fusion.2 = (f32[4,2,256]{2,1,0:T(2,128)S(1)}, f32[4,2048,256,2]{2,1,3,0:T(8,128)}) fusion(bf16[256,4,2,64]{0,3,2,1:T(8,128)(2,1)S(1)} %get-tuple-element.194, bf16[2,2048,4,64]{1,3,2,0:T(8,128)(2,1)} %get-tuple-element.193, s32[]{:T(128)} %get-tuple-element.180), kind=kOutput, calls=%fused_computation.1.clone.1 | convolution fusion | flops 541063168 | bytes 18096640 | tf_op jit(solution)/shard_map/while/body/eval_jaxpr/qhgd,khd->hgqk/dot_general | solution.py:112
  184.9 7.6 %fusion.55 = f32[256,4,2,64]{0,3,2,1:T(8,128)S(1)} fusion(f32[4,2048,256,2]{2,1,3,0:T(8,128)} %get-tuple-element.169, f32[4,2,256]{2,1,0:T(2,128)S(1)} %get-tuple-element.190, bf16[2,2048,4,64]{1,3,2,0:T(8,128)(2,1)} %get-tuple-element.195, s32[]{:T(128)} %get-tuple-element.180, f32[256,4,2,64]{0,3,2,1:T(8,128)S(1)} %get-tuple-element.183, ...), kind=kOutput, calls=%fused_computation.8.clone.1 | convolution fusion | flops 545652736 | bytes 18891264 | tf_op jit(solution)/shard_map/while/body/eval_jaxpr/hgqk,khd->qhgd/dot_general | solution.py:119
  192.5 8.0 %fusion.53 = f32[4,2,256]{2,1,0:T(2,128)S(1)} fusion(f32[4,2048,256,2]{2,1,3,0:T(8,128)} %get-tuple-element.169, f32[4,2,256]{2,1,0:T(2,128)S(1)} %get-tuple-element.190), kind=kLoop, calls=%fused_computation.4.clone.1 | loop fusion | flops 8386560 | bytes 16793600 | tf_op jit(solution)/shard_map/while/body/eval_jaxpr/reduce_sum | solution.py:118
  200.6 1.7 convolution_convert_fusion.1
  202.3 0.0 all-reduce.3.cloned.1.call-update
  202.4 0.0 all-gather.11.cloned.1.call-start
  202.4 0.5 all-gather.11.cloned.1.call-update
  202.9 0.0 all-gather.9.cloned.1.call-start
  203.0 0.5 all-gather.9.cloned.1.call-update
  203.5 0.0 copy-start.2
  203.5 0.0 copy-start.3
  203.6 0.2 reduce-scatter.2.cloned.1.call-start
  203.8 18.7 %all-reduce.3.cloned.1.call-done = bf16[256,2048]{1,0:T(8,128)(2,1)} async-done(((bf16[256,2048]{1,0:T(8,128)(2,1)}), bf16[256,2048]{1,0:T(8,128)(2,1)}) %all-reduce.3.cloned.1.call-update) | async-done | bytes 1048592 | tf_op jit(solution)/shard_map/psum | solution.py:138
  222.4 2.0 fusion.24
  224.5 1.8 multiply_reduce_fusion
  226.3 2.8 add_convert_fusion
  229.2 242.9 %all-gather.11.cloned.1.call-done = bf16[4096,2048]{1,0:T(8,128)(2,1)} async-done(((bf16[4096,128]{1,0:T(8,128)(2,1)}), bf16[4096,2048]{1,0:T(8,128)(2,1)}) %all-gather.11.cloned.1.call-update) | async-done | bytes 16777232 | tf_op jit(solution)/shard_map/all_gather | solution.py:151
  472.0 191.8 %all-gather.9.cloned.1.call-done = bf16[2048,4096]{1,0:T(8,128)(2,1)} async-done(((bf16[128,4096]{1,0:T(8,128)(2,1)}), bf16[2048,4096]{1,0:T(8,128)(2,1)}) %all-gather.9.cloned.1.call-update) | async-done | bytes 16777232 | tf_op jit(solution)/shard_map/all_gather | solution.py:145
  663.9 16.5 %convolution_convert_fusion = bf16[256,2048]{1,0:T(8,128)(2,1)} fusion(bf16[4096,2048]{1,0:T(8,128)(2,1)} %all-gather.11.cloned.1.call-done, bf16[256,2048]{1,0:T(8,128)(2,1)} %add_convert_fusion, bf16[2048,4096]{1,0:T(8,128)(2,1)} %all-gather.9.cloned.1.call-done), kind=kOutput, calls=%fused_computation.26 | convolution fusion | flops 8593604608 | bytes 35651584 | tf_op jit(solution)/shard_map/dot_general | solution.py:149
  680.3 0.0 reduce-scatter.2.cloned.1.call-update
  680.4 9.9 %reduce-scatter.2.cloned.1.call-done = bf16[256,1024]{1,0:T(8,128)(2,1)} async-done(((bf16[256,2048]{1,0:T(8,128)(2,1)}), bf16[256,1024]{1,0:T(8,128)(2,1)}) %reduce-scatter.2.cloned.1.call-update) | async-done | bytes 524304 | tf_op jit(solution)/shard_map/reduce_scatter | solution.py:154
  690.4 1.5 fusion.25
  691.9 2.5 all-reduce
  694.4 2.3 add_convert_fusion.1
  (33 shorter events, 0.4 us)
Async XLA Ops:
  6.5 194.1 %copy-start = (bf16[512,2048]{1,0:T(8,128)(2,1)S(1)}, bf16[512,2048]{1,0:T(8,128)(2,1)}, u32[]{:S(2)}) copy-start(bf16[512,2048]{1,0:T(8,128)(2,1)} %param.20) | copy-start | bytes 6291460
  6.5 4.9 copy-start.6
  6.5 65.8 %all-gather.5.cloned.1.call-start = ((), (), s32[]{:S(2)}) async-start(), calls=%async_computation.1 | async-start | bytes 2228224 | tf_op jit(solution)/shard_map/all_gather | solution.py:103
  9.5 127.1 %all-gather.7.cloned.1.call-start = ((), (), s32[]{:S(2)}) async-start(), calls=%async_computation.2 | async-start | bytes 2228224 | tf_op jit(solution)/shard_map/all_gather | solution.py:104
  10.2 212.2 %all-reduce.3.cloned.1.call-start = ((), (), s32[]{:S(2)}) async-start(), calls=%async_computation.3 | async-start | bytes 2097152 | tf_op jit(solution)/shard_map/psum | solution.py:138
  202.4 269.7 %all-gather.11.cloned.1.call-start = ((), (), s32[]{:S(2)}) async-start(), calls=%async_computation.5 | async-start | bytes 17825792 | tf_op jit(solution)/shard_map/all_gather | solution.py:151
  202.9 460.9 %all-gather.9.cloned.1.call-start = ((), (), s32[]{:S(2)}) async-start(), calls=%async_computation.4 | async-start | bytes 17825792 | tf_op jit(solution)/shard_map/all_gather | solution.py:145
  203.5 22.8 %copy-start.2 = (f32[2048]{0:T(1024)S(1)}, f32[2048]{0:T(1024)}, u32[]{:S(2)}) copy-start(f32[2048]{0:T(1024)} %param.23) | copy-start | bytes 24580
  203.5 22.8 %copy-start.3 = (f32[2048]{0:T(1024)S(1)}, f32[2048]{0:T(1024)}, u32[]{:S(2)}) copy-start(f32[2048]{0:T(1024)} %param.22) | copy-start | bytes 24580
  203.6 486.8 %reduce-scatter.2.cloned.1.call-start = ((), (), s32[]{:S(2)}) async-start(), calls=%async_computation.6 | async-start | bytes 1572864 | tf_op jit(solution)/shard_map/reduce_scatter | solution.py:154
  222.4 2.1 copy-start.1
  229.2 451.2 %copy-start.4 = (f32[2048]{0:T(1024)S(1)}, f32[2048]{0:T(1024)}, u32[]{:S(2)}) copy-start(f32[2048]{0:T(1024)} %param.26) | copy-start | bytes 24580
  229.2 451.2 %copy-start.5 = (f32[2048]{0:T(1024)S(1)}, f32[2048]{0:T(1024)}, u32[]{:S(2)}) copy-start(f32[2048]{0:T(1024)} %param.27) | copy-start | bytes 24580
Sparse Core Ops, SparseCore 0:
  10.1 62.2 all-gather.4
  75.1 61.4 all-gather.6
  202.5 19.9 all-reduce.2
  225.0 246.9 all-gather.10
  474.7 189.1 all-gather.8
  680.5 9.8 reduce-scatter.1
where the time goes:
time: 705 us; the launch traced here: 704 us
  waiting for transfers between devices  582 us (83%)
  matrix products  52 us (7%)
  other arithmetic  28.7 us (4%)
  local copies, waits for them, and re-layouts  24.6 us (3%)
  between operations  13.7 us (2%)
    all_gather x1, waiting for transfers between devices, local(): lax.all_gather(down_weight, 'sp', axis=1, tiled=True)  243 us
    all_gather x1, waiting for transfers between devices, local(): lax.all_gather(up_weight, 'sp', axis=0, tiled=True)  192 us
    all_gather x1, waiting for transfers between devices, local(): key_piece = lax.all_gather(k_sent, 'sp', axis=0, tiled=True)  60.6 us
    all_gather x1, waiting for transfers between devices, local(): value_piece = lax.all_gather(values, 'sp', axis=0, tiled=True)  56 us
    dot_general x2, matrix products, advance(): jnp.einsum('qhgd,khd->hgqk', q_grouped, blocks[0], preferred_element_type...  18.7 us
    psum x1, waiting for transfers between devices, local(): lax.psum(partial_value.astype(jnp.bfloat16), 'tp').astype(jnp.float32)  18.7 us
    dot_general x1, matrix products, local(): jnp.dot(hidden, lax.all_gather(down_weight, 'sp', axis=1, tiled=True), pr...  16.5 us
    reduce_sum x2, other arithmetic, advance(): totals = totals * factor + jnp.sum(weights, -1)  16 us
  transfers between devices with their start and end apart: 6, of which 6 were waited for; matrix products, arithmetic and copies ran while one was open for 2% of the time, Pallas kernels for 0%

commit v1 on v0

v1 whole, which is shorter than its diff:
```python
import math

import jax
import jax.numpy as jnp
from jax import lax
from jax.experimental import pallas as pl
from jax.experimental.pallas import tpu as pltpu
from jax.sharding import PartitionSpec as P

D = 2048
HEAD_SIZE = 64
GRID_W = 64


ALPHA = 8.0**0.25
ROTARY_BASE = 10000.0
RMS_EPSILON = 1e-06
NORM_EPSILON = 1e-05


def rotate_grid(heads_in, grid_places):
    half_dim = heads_in.shape[-1] // 2
    quarter = half_dim // 2
    inverse = ROTARY_BASE ** (-jnp.arange(quarter, dtype=jnp.float32) / quarter)

    def spin(segment, coords):
        angles = coords.astype(jnp.float32)[:, None] * inverse[None, :]
        cos_val = jnp.cos(angles)[:, None, :]
        sin_val = jnp.sin(angles)[:, None, :]
        lead_half = segment[..., :quarter]
        tail_half = segment[..., quarter:]
        return jnp.concatenate(
            [lead_half * cos_val - tail_half * sin_val, tail_half * cos_val + lead_half * sin_val],
            -1,
        )

    return jnp.concatenate(
        [
            spin(heads_in[..., :half_dim], grid_places // GRID_W),
            spin(heads_in[..., half_dim:], grid_places % GRID_W),
        ],
        -1,
    )


def prepare_inputs(heads_in, gain_vec, grid_places, factor):
    values32 = heads_in.astype(jnp.float32)
    normed = (
        values32
        * lax.rsqrt(jnp.mean(values32 * values32, -1, keepdims=True) + RMS_EPSILON)
        * gain_vec
    )
    return (rotate_grid(normed, grid_places) * factor).astype(jnp.bfloat16)


def layer_norm(pre_norm, gain_vec, bias_vec):
    row_mean = jnp.mean(pre_norm, -1, keepdims=True)
    centred = pre_norm - row_mean
    spread = jnp.mean(centred * centred, -1, keepdims=True)
    return centred * lax.rsqrt(spread + NORM_EPSILON) * gain_vec + bias_vec


def finish_norm(pre_norm, stats, gain_vec, bias_vec):
    row_mean = stats[0][:, None] / D
    spread = stats[1][:, None] / D - row_mean * row_mean
    return (pre_norm - row_mean) * lax.rsqrt(spread + NORM_EPSILON) * gain_vec + bias_vec


def take_cols(array_in, col_start, col_width):
    return lax.dynamic_slice_in_dim(array_in, col_start, col_width, array_in.ndim - 1)


def swap(array_in, axis_name, offset):
    size = lax.axis_size(axis_name)
    return lax.ppermute(array_in, axis_name, [(i, i ^ offset) for i in range(size)])


def gather_low(array_in, low_count, ascending=True):
    bits = [1 << b for b in range(low_count.bit_length() - 1)]
    slots = {0: array_in}
    for bit in bits if ascending else bits[::-1]:
        order = sorted(slots)
        got = swap(jnp.stack([slots[e] for e in order], 0), "sp", bit)
        for n, e in enumerate(order):
            slots[e ^ bit] = got[n]
    return jnp.stack([slots[e] for e in range(low_count)], 0)


def attend_kernel(q_ref, kv_ref, o_ref):
    k = kv_ref[:, :HEAD_SIZE]
    outs = []
    for g in range(q_ref.shape[1] // HEAD_SIZE):
        q = q_ref[:, g * HEAD_SIZE : (g + 1) * HEAD_SIZE]
        scores = lax.dot_general(
            q, k, (((1,), (1,)), ((), ())), preferred_element_type=jnp.float32
        )
        weights = jnp.exp(scores - jnp.max(scores, -1, keepdims=True))
        totals = jnp.sum(weights, -1, keepdims=True)
        summed = jnp.dot(
            weights.astype(jnp.bfloat16), kv_ref[...], preferred_element_type=jnp.float32
        )
        outs.append(summed[:, HEAD_SIZE:] / totals)
    o_ref[...] = jnp.concatenate(outs, 1).astype(jnp.bfloat16)


def attend(q_rows, kv_rows):
    rows, width = q_rows.shape
    keys = kv_rows.shape[0]
    block = math.gcd(rows, max(16, (1 << 20) // keys))
    return pl.pallas_call(
        attend_kernel,
        grid=(rows // block,),
        in_specs=[
            pl.BlockSpec((block, width), lambda i: (i, 0)),
            pl.BlockSpec((keys, kv_rows.shape[1]), lambda i: (0, 0)),
        ],
        out_specs=pl.BlockSpec((block, width), lambda i: (i, 0)),
        out_shape=jax.ShapeDtypeStruct((rows, width), jnp.bfloat16),
    )(q_rows, kv_rows)


def local(
    queries,
    keys,
    values,
    q_gain,
    key_norm_gain,
    out_weight,
    residual,
    ln1_gain,
    ln1_bias,
    up_weight,
    down_weight,
    ln2_gain,
    ln2_bias,
):
    n_sp = lax.axis_size("sp")
    n_tp = lax.axis_size("tp")
    split = math.gcd(n_sp, 4)
    low_count = n_sp // split
    me = lax.axis_index("sp")
    hi = me // low_count
    core = lax.axis_index("tp")

    tok_rows = queries.shape[0]
    grid_places = me * tok_rows + jnp.arange(tok_rows, dtype=jnp.int32)
    kv_heads = keys.shape[1] // HEAD_SIZE
    q_count = queries.shape[1] // HEAD_SIZE
    group = q_count // kv_heads
    q_sent = prepare_inputs(
        queries.reshape(tok_rows, q_count, HEAD_SIZE), q_gain, grid_places, HEAD_SIZE ** (-0.5)
    ).reshape(tok_rows, kv_heads, group * HEAD_SIZE)
    k_sent = prepare_inputs(
        keys.reshape(tok_rows, kv_heads, HEAD_SIZE), key_norm_gain, grid_places, 1.0
    )
    v_sent = values.reshape(tok_rows, kv_heads, HEAD_SIZE)
    packed = jnp.concatenate([q_sent, k_sent, v_sent], -1)
    packed = jnp.transpose(packed, (1, 0, 2))
    q_width = group * HEAD_SIZE

    if kv_heads % split == 0:
        per = kv_heads // split
        parts = []
        for d in range(split):
            block = lax.dynamic_slice_in_dim(packed, (hi ^ d) * per, per, 0)
            parts.append(block if d == 0 else swap(block, "sp", d * low_count))
        got = jnp.concatenate(parts, 1)
        kv_all = gather_low(got[..., q_width:], low_count)
        heads_out = []
        for h in range(per):
            kv_rows = kv_all[:, h].reshape(-1, 2 * HEAD_SIZE)
            heads_out.append(attend(got[h, :, :q_width], kv_rows))
        att = jnp.concatenate(heads_out, 1)
        width = att.shape[1]
        attended = jnp.zeros((tok_rows, split * width), jnp.bfloat16)
        for d in range(split):
            block = att[d * tok_rows : (d + 1) * tok_rows]
            if d:
                block = swap(block, "sp", d * low_count)
            attended = lax.dynamic_update_slice_in_dim(attended, block, (hi ^ d) * width, 1)
    else:
        kv_all = lax.all_gather(packed[..., q_width:], "sp", axis=1, tiled=True)
        attended = jnp.concatenate(
            [attend(packed[h, :, :q_width], kv_all[h]) for h in range(kv_heads)], 1
        )

    ff_own = up_weight.shape[1] // split
    up_parts, down_parts = [], []
    for d in range(split):
        start = (hi ^ d) * ff_own
        up_block = lax.dynamic_slice_in_dim(up_weight, start, ff_own, 1)
        down_block = lax.dynamic_slice_in_dim(down_weight, start, ff_own, 0)
        if d:
            up_block = swap(up_block, "sp", d * low_count)
            down_block = swap(down_block, "sp", d * low_count)
        up_parts.append(up_block)
        down_parts.append(down_block)
    up_all = gather_low(jnp.stack(up_parts, 0), low_count)
    down_all = gather_low(jnp.stack(down_parts, 0), low_count, ascending=False)

    def placed(pieces, axis):
        ordered = []
        for s in range(n_sp):
            rel = me ^ s
            piece = lax.dynamic_slice(
                pieces,
                (rel % low_count, rel // low_count, 0, 0),
                (1, 1) + pieces.shape[2:],
            )
            ordered.append(piece.reshape(pieces.shape[2:]))
        return jnp.concatenate(ordered, axis)

    up_own = placed(up_all, 0)
    down_own = placed(down_all, 1)

    mixed_sum = jnp.zeros((tok_rows, D), jnp.float32)
    for d in range(n_tp):
        att_d = attended if d == 0 else swap(attended, "tp", d)
        w_d = out_weight if d == 0 else swap(out_weight, "tp", d)
        partial_value = jnp.dot(att_d, w_d, preferred_element_type=jnp.float32)
        mixed_sum = mixed_sum + partial_value.astype(jnp.bfloat16).astype(jnp.float32)
    full_rows = layer_norm(
        ALPHA * residual.astype(jnp.float32) + mixed_sum, ln1_gain, ln1_bias
    ).astype(jnp.bfloat16)

    col_width = D // n_tp
    normed_own = take_cols(full_rows, core * col_width, col_width)

    ffn_cols = jnp.zeros((tok_rows, col_width), jnp.float32)
    for d in range(split):
        if d == 0:
            rows_d = full_rows
        else:
            mine = swap(normed_own, "sp", d * low_count)
            rows_d = jnp.zeros((tok_rows, D), jnp.bfloat16)
            for e in range(n_tp):
                piece = mine if e == 0 else swap(mine, "tp", e)
                rows_d = lax.dynamic_update_slice_in_dim(
                    rows_d, piece, (core ^ e) * col_width, 1
                )
        up_acts = jnp.dot(rows_d, up_own, preferred_element_type=jnp.float32)
        hidden = jnp.square(jnp.maximum(up_acts, 0.0)).astype(jnp.bfloat16)
        partial_ffn = jnp.dot(hidden, down_own, preferred_element_type=jnp.float32).astype(
            jnp.bfloat16
        )
        cols = jnp.zeros((tok_rows, col_width), jnp.float32)
        for e in range(n_tp):
            piece = take_cols(partial_ffn, (core ^ e) * col_width, col_width)
            if e:
                piece = swap(piece, "tp", e)
            cols = cols + piece.astype(jnp.float32)
        if d:
            cols = swap(cols.astype(jnp.bfloat16), "sp", d * low_count).astype(jnp.float32)
        ffn_cols = ffn_cols + cols

    second = ALPHA * normed_own.astype(jnp.float32) + ffn_cols
    stats_two = lax.psum((jnp.sum(second, -1), jnp.sum(second * second, -1)), "tp")
    return finish_norm(
        second,
        stats_two,
        take_cols(ln2_gain, core * col_width, col_width),
        take_cols(ln2_bias, core * col_width, col_width),
    ).astype(jnp.bfloat16)


def solution(mesh):
    return jax.shard_map(
        local,
        mesh=mesh,
        in_specs=(
            P("sp", "tp"),
            P("sp", "tp"),
            P("sp", "tp"),
            P(),
            P(),
            P("tp", None),
            P("sp", None),
            P(),
            P(),
            P("sp", "tp"),
            P("tp", "sp"),
            P(),
            P(),
        ),
        out_specs=P("sp", "tp"),
        check_vma=False,
    )
```

time: 705 us -> 278 us (0.39)
  waiting for transfers between devices: 582 us -> 127 us
  starting transfers between devices: 0.38 us -> 45.9 us
  matrix products: 52 us -> 31.3 us
  Pallas kernels: 0 us -> 14.9 us
  between operations: 13.7 us -> 0.79 us
  local copies, waits for them, and re-layouts: 24.6 us -> 35.6 us
  other arithmetic: 28.7 us -> 18.3 us
    all_gather x4 -> x0, waiting for transfers between devices: 551 us -> none  [the longest x1 243 us: local(): lax.all_gather(down_weight, 'sp', axis=1, tiled=True)]
    ppermute x0 -> x33, waiting for transfers between devices: none -> 127 us  [swap(): lax.ppermute(array_in, axis_name, [(i, i ^ offset) for i in range(size)])]
    ppermute x0 -> x33, starting transfers between devices: none -> 45.9 us  [swap(): lax.ppermute(array_in, axis_name, [(i, i ^ offset) for i in range(size)])]
    dot_general x6, matrix products: 52 us -> 31.3 us  [the longest x4 26.4 us: local(): jnp.dot(hidden, down_own, preferred_element_type=jnp.float32)]
    psum x1 -> x0, waiting for transfers between devices: 18.7 us -> none  [local(): lax.psum(partial_value.astype(jnp.bfloat16), 'tp').astype(jnp.float32)]
    reduce_sum x3 -> x0, other arithmetic: 18 us -> none  [the longest x2 16 us: advance(): totals = totals * factor + jnp.sum(weights, -1)]
    pallas_call x0 -> x1, Pallas kernels: none -> 14.9 us  [attend(): pl.pallas_call(attend_kernel, grid=(rows // block,), in_specs=[pl.BlockSp...]
    reshape x2 -> x0, local copies, waits for them, and re-layouts: 11.5 us -> none  [the longest x1 7.06 us: local(): value_piece.reshape(key_count // block_len, block_len, kv_heads, HEAD_SIZE)]
  transfers between devices with their start and end apart: 6 -> 33, of which waited for: 6 -> 16; matrix products, arithmetic and copies ran while one was open for 2% -> 16% of each run, Pallas kernels for 0% -> 5%
where the time goes in v1:
time: 278 us; the launch traced here: 277 us
  waiting for transfers between devices  127 us (46%)
  starting transfers between devices  45.9 us (17%)
  local copies, waits for them, and re-layouts  35.6 us (13%)
  matrix products  31.3 us (11%)
  other arithmetic  18.3 us (7%)
  Pallas kernels  14.9 us (5%)
  blocking collectives  3.44 us (1%)
    ppermute x33, waiting for transfers between devices, swap(): lax.ppermute(array_in, axis_name, [(i, i ^ offset) for i in range(size)])  127 us
    ppermute x33, starting transfers between devices, swap(): lax.ppermute(array_in, axis_name, [(i, i ^ offset) for i in range(size)])  45.9 us
    dot_general x4, matrix products, local(): jnp.dot(hidden, down_own, preferred_element_type=jnp.float32)  26.4 us
    unnamed x72, local copies, waits for them, and re-layouts  17.1 us
    pallas_call x1, Pallas kernels, attend(): pl.pallas_call(attend_kernel, grid=(rows // block,), in_specs=[pl.BlockSp...  14.9 us
    another operation x5, other arithmetic, gather_low(): return jnp.stack([slots[e] for e in range(low_count)], 0)  6.03 us
    dynamic_update_slice x6, local copies, waits for them, and re-layouts, local(): lax.dynamic_update_slice_in_dim(rows_d, piece, (core ^ e) * col_width, 1)  5.93 us
    dynamic_slice x9, local copies, waits for them, and re-layouts, take_cols(): lax.dynamic_slice_in_dim(array_in, col_start, col_width, array_in.ndim - 1)  5.83 us
  transfers between devices with their start and end apart: 33, of which 16 were waited for; matrix products, arithmetic and copies ran while one was open for 16% of the time, Pallas kernels for 5%

profile of v1, /device:TPU:9, one launch (start us, length us, event | category | flops | bytes accessed | tf_op | source)
XLA Modules:
  0.0 276.8 jit_solution(13906992168843164408)
XLA Ops:
  3.3 2.5 collective-permute-start.1
  6.2 1.5 collective-permute-start.9
  7.8 3.6 %collective-permute-done.1 = bf16[1,256,256]{2,1,0:T(8,128)(2,1)S(1)} collective-permute-done((bf16[1,256,256]{2,1,0:T(8,128)(2,1)S(1)}, bf16[1,256,256]{2,1,0:T(8,128)(2,1)S(1)}, u32[]{:S(2)}, u32[]{:S(2)}) %collective-permute-start.1) | collective-permute-done | bytes 131104 | tf_op jit(solution)/shard_map/ppermute | solution.py:75
  11.4 5.8 %collective-permute-done.2 = bf16[1,256,256]{2,1,0:T(8,128)(2,1)S(1)} collective-permute-done((bf16[1,256,256]{2,1,0:T(8,128)(2,1)S(1)}, bf16[1,256,256]{2,1,0:T(8,128)(2,1)S(1)}, u32[]{:S(2)}, u32[]{:S(2)}) %collective-permute-start.2) | collective-permute-done | bytes 131104 | tf_op jit(solution)/shard_map/ppermute | solution.py:75
  19.4 2.6 collective-permute-start.11
  22.1 2.0 collective-permute-done.3
  25.1 1.4 collective-permute-done.10
  27.7 4.6 %collective-permute-done.11 = bf16[128,1024]{1,0:T(8,128)(2,1)S(1)} collective-permute-done((bf16[128,1024]{1,0:T(8,128)(2,1)S(1)}, bf16[128,1024]{1,0:T(8,128)(2,1)S(1)}, u32[]{:S(2)}, u32[]{:S(2)}) %collective-permute-start.11) | collective-permute-done | bytes 262176 | tf_op jit(solution)/shard_map/ppermute | solution.py:75
  32.3 12.0 %collective-permute-done.12 = bf16[128,1024]{1,0:T(8,128)(2,1)S(1)} collective-permute-done((bf16[128,1024]{1,0:T(8,128)(2,1)S(1)}, bf16[128,1024]{1,0:T(8,128)(2,1)S(1)}, u32[]{:S(2)}, u32[]{:S(2)}) %collective-permute-start.12) | collective-permute-done | bytes 262176 | tf_op jit(solution)/shard_map/ppermute | solution.py:75
  44.3 2.7 collective-permute-start.17
  47.5 12.4 %collective-permute-done.16 = bf16[1024,128]{1,0:T(8,128)(2,1)S(1)} collective-permute-done((bf16[1024,128]{1,0:T(8,128)(2,1)S(1)}, bf16[1024,128]{1,0:T(8,128)(2,1)S(1)}, u32[]{:S(2)}, u32[]{:S(2)}) %collective-permute-start.16) | collective-permute-done | bytes 262176 | tf_op jit(solution)/shard_map/ppermute | solution.py:75
  59.8 5.8 %collective-permute-done.17 = bf16[1024,128]{1,0:T(8,128)(2,1)S(1)} collective-permute-done((bf16[1024,128]{1,0:T(8,128)(2,1)S(1)}, bf16[1024,128]{1,0:T(8,128)(2,1)S(1)}, u32[]{:S(2)}, u32[]{:S(2)}) %collective-permute-start.17) | collective-permute-done | bytes 262176 | tf_op jit(solution)/shard_map/ppermute | solution.py:75
  67.1 2.2 pad_maximum_fusion.4
  69.3 14.9 %shard_map.127 = bf16[1024,128]{1,0:T(8,128)(2,1)} custom-call(bf16[1024,128]{1,0:T(8,128)(2,1)} %get-tuple-element.25.q_ref, bf16[4096,128]{1,0:T(8,128)(2,1)} %bitcast.115), custom_call_target="tpu_custom_call" | custom-call | tf_op jit(solution)/shard_map/pallas_call | solution.py:110
  84.2 1.6 fusion.30
  85.8 3.2 %collective-permute-start.6 = (bf16[256,128]{1,0:T(8,128)(2,1)S(1)}, bf16[256,128]{1,0:T(8,128)(2,1)S(1)}, u32[]{:S(2)}, u32[]{:S(2)}) collective-permute-start(bf16[256,128]{1,0:T(8,128)(2,1)S(1)} %get-tuple-element.33), channel_id=1, source_target_pairs={{0,16},{2,18},{4,20},{6,22},{8,24},{10,26},{12,28},{14,30},{16,0},... | collective-permute-start | bytes 196616 | tf_op jit(solution)/shard_map/ppermute | solution.py:75
  89.5 2.0 collective-permute-start.7
  92.4 1.9 collective-permute-done.7
  94.3 4.5 %collective-permute-start.8 = (bf16[256,512]{1,0:T(8,128)(2,1)S(1)}, bf16[256,512]{1,0:T(8,128)(2,1)S(1)}, u32[]{:S(2)}, u32[]{:S(2)}) collective-permute-start(bf16[256,512]{1,0:T(8,128)(2,1)S(1)} %constant_dynamic-update-slice_fusion.11), channel_id=1, source_target_pairs={{0,1},{1,0},{2,3},{3,2},{4,5},{5,4},{6,7},{7,6},{8,9},{9,8},{10,11... | collective-permute-start | bytes 786440 | tf_op jit(solution)/shard_map/ppermute | solution.py:75
  98.8 1.7 pad_maximum_fusion.2
  100.7 2.8 %pad_maximum_fusion.3 = bf16[2,4,1024,128]{3,2,1,0:T(8,128)(2,1)} fusion(bf16[1,4,1024,128]{3,2,1,0:T(8,128)(2,1)} %collective-permute-done.18, bf16[1,4,1024,128]{3,2,1,0:T(8,128)(2,1)S(1)} %maximum_bitcast_fusion.1), kind=kLoop, calls=%fused_computation.13 | loop fusion | flops 1048576 | bytes 4194304 | tf_op jit(solution)/shard_map/stack | solution.py:83
  103.8 2.3 fusion.3
  106.2 2.5 fusion.31
  111.4 1.4 collective-permute-start.25
  113.1 19.9 %collective-permute-done.21 = bf16[256,1024]{1,0:T(8,128)(2,1)} collective-permute-done((bf16[256,1024]{1,0:T(8,128)(2,1)}, bf16[256,1024]{1,0:T(8,128)(2,1)}, u32[]{:S(2)}, u32[]{:S(2)}) %collective-permute-start.21) | collective-permute-done | bytes 524320 | tf_op jit(solution)/shard_map/ppermute | solution.py:75
  133.0 1.4 collective-permute-start.22
  134.3 1.8 collective-permute-done.25
  136.2 12.5 %collective-permute-start.26 = (bf16[256,1024]{1,0:T(8,128)(2,1)}, bf16[256,1024]{1,0:T(8,128)(2,1)}, u32[]{:S(2)}, u32[]{:S(2)}) collective-permute-start(bf16[256,1024]{1,0:T(8,128)(2,1)} %collective-permute-done.25), channel_id=1, source_target_pairs={{0,1},{1,0},{2,3},{3,2},{4,5},{5,4},{6,7},{7,6},{8,9},{9,8},{10,11... | collective-permute-start | bytes 1572872 | tf_op jit(solution)/shard_map/ppermute | solution.py:75
  148.7 9.8 %collective-permute-done.29 = bf16[256,1024]{1,0:T(8,128)(2,1)} collective-permute-done((bf16[256,1024]{1,0:T(8,128)(2,1)}, bf16[256,1024]{1,0:T(8,128)(2,1)}, u32[]{:S(2)}, u32[]{:S(2)}) %collective-permute-start.29) | collective-permute-done | bytes 524320 | tf_op jit(solution)/shard_map/ppermute | solution.py:75
  158.5 1.6 collective-permute-start.30
  164.9 1.5 constant_dynamic-update-slice_fusion.7
  168.4 1.8 pad_maximum_fusion
  170.2 1.7 fusion.29
  171.9 1.8 pad_maximum_fusion.1
  185.5 2.0 copy-done.15
  188.3 6.9 %convolution_convert_fusion.5 = bf16[256,2048]{1,0:T(8,128)(2,1)} fusion(bf16[1024,2048]{1,0:T(8,128)(2,1)} %bitcast_dynamic-update-slice_fusion, bf16[256,2048]{1,0:T(8,128)(2,1)S(1)} %add_convert_fusion, bf16[2048,1024]{1,0:T(8,128)(2,1)} %copy-done.15), kind=kOutput, calls=%fused_computation.7 | convolution fusion | flops 2148794368 | bytes 10485760 | tf_op jit(solution)/shard_map/dot_general | solution.py:243
  195.3 6.8 %convolution_convert_fusion.4 = bf16[256,2048]{1,0:T(8,128)(2,1)} fusion(bf16[1024,2048]{1,0:T(8,128)(2,1)} %bitcast_dynamic-update-slice_fusion, bf16[256,2048]{1,0:T(8,128)(2,1)S(1)} %copy-done.7, bf16[2048,1024]{1,0:T(8,128)(2,1)} %copy-done.15), kind=kOutput, calls=%fused_computation.6 | convolution fusion | flops 2148794368 | bytes 10485760 | tf_op jit(solution)/shard_map/dot_general | solution.py:243
  202.1 1.9 constant_dynamic-slice_fusion.2
  204.0 6.9 %convolution_convert_fusion.3 = bf16[256,2048]{1,0:T(8,128)(2,1)} fusion(bf16[1024,2048]{1,0:T(8,128)(2,1)} %bitcast_dynamic-update-slice_fusion, bf16[256,2048]{1,0:T(8,128)(2,1)S(1)} %copy-done.9, bf16[2048,1024]{1,0:T(8,128)(2,1)} %copy-done.15), kind=kOutput, calls=%fused_computation.5 | convolution fusion | flops 2148794368 | bytes 10485760 | tf_op jit(solution)/shard_map/dot_general | solution.py:243
  210.9 1.9 constant_dynamic-slice_fusion.1
  213.2 5.8 %convolution_convert_fusion.2 = bf16[256,2048]{1,0:T(8,128)(2,1)S(1)} fusion(bf16[1024,2048]{1,0:T(8,128)(2,1)} %bitcast_dynamic-update-slice_fusion, bf16[256,2048]{1,0:T(8,128)(2,1)S(1)} %copy-done.5, bf16[2048,1024]{1,0:T(8,128)(2,1)} %copy-done.15), kind=kOutput, calls=%fused_computation.4 | convolution fusion | flops 2148794368 | bytes 10485760 | tf_op jit(solution)/shard_map/dot_general | solution.py:243
  220.8 1.4 add_convert_fusion.4
  222.3 1.4 add_convert_fusion.3
  223.7 2.3 collective-permute-start.28
  226.6 16.5 %collective-permute-done.24 = bf16[256,1024]{1,0:T(8,128)(2,1)S(1)} collective-permute-done((bf16[256,1024]{1,0:T(8,128)(2,1)S(1)}, bf16[256,1024]{1,0:T(8,128)(2,1)S(1)}, u32[]{:S(2)}, u32[]{:S(2)}) %collective-permute-start.24) | collective-permute-done | bytes 524320 | tf_op jit(solution)/shard_map/ppermute | solution.py:75
  243.1 16.2 %collective-permute-done.28 = bf16[256,1024]{1,0:T(8,128)(2,1)S(1)} collective-permute-done((bf16[256,1024]{1,0:T(8,128)(2,1)S(1)}, bf16[256,1024]{1,0:T(8,128)(2,1)S(1)}, u32[]{:S(2)}, u32[]{:S(2)}) %collective-permute-start.28) | collective-permute-done | bytes 524320 | tf_op jit(solution)/shard_map/ppermute | solution.py:75
  259.3 12.3 %collective-permute-done.32 = bf16[256,1024]{1,0:T(8,128)(2,1)S(1)} collective-permute-done((bf16[256,1024]{1,0:T(8,128)(2,1)S(1)}, bf16[256,1024]{1,0:T(8,128)(2,1)S(1)}, u32[]{:S(2)}, u32[]{:S(2)}) %collective-permute-start.32) | collective-permute-done | bytes 524320 | tf_op jit(solution)/shard_map/ppermute | solution.py:75
  272.3 3.4 %all-reduce = (f32[256]{0:T(256)S(1)}, f32[256]{0:T(256)S(1)}) all-reduce(f32[256]{0:T(256)S(1)} %get-tuple-element.6, f32[256]{0:T(256)S(1)} %get-tuple-element.5), channel_id=1, replica_groups=mesh['sp'=16,'tp'=2] {'tp'}, use_global_device_ids=true, to_apply=%region_7.8 | all-reduce | flops 512 | bytes 4096 | tf_op jit(solution)/shard_map/psum | solution.py:257
  (167 shorter events, 38.5 us)
Async XLA Ops:
  0.0 2.8 %copy-start.14 = (bf16[256,256]{1,0:T(8,128)(2,1)S(1)}, bf16[256,256]{1,0:T(8,128)(2,1)}, u32[]{:S(2)}) copy-start(bf16[256,256]{1,0:T(8,128)(2,1)} %param.15) | copy-start | bytes 393220
  2.3 17.0 %copy-start.2 = (bf16[128,4096]{1,0:T(8,128)(2,1)S(1)}, bf16[128,4096]{1,0:T(8,128)(2,1)}, u32[]{:S(2)}) copy-start(bf16[128,4096]{1,0:T(8,128)(2,1)} %param.22) | copy-start | bytes 3145732
  2.5 19.6 %copy-start.3 = (bf16[4096,128]{1,0:T(8,128)(2,1)S(1)}, bf16[4096,128]{1,0:T(8,128)(2,1)}, u32[]{:S(2)}) copy-start(bf16[4096,128]{1,0:T(8,128)(2,1)} %param.23) | copy-start | bytes 3145732
  3.2 4.7 %collective-permute-start = (bf16[1,256,256]{2,1,0:T(8,128)(2,1)S(1)}, bf16[1,256,256]{2,1,0:T(8,128)(2,1)S(1)}, u32[]{:S(2)}, u32[]{:S(2)}) collective-permute-start(bf16[1,256,256]{2,1,0:T(8,128)(2,1)S(1)} %bitcast.125), channel_id=1, source_target_pairs={{0,8},{2,10},{4,12},{6,14},{8,0},{10,2},{12,4},{14,6},{16,24},{18,... | collective-permute-start | bytes 393224 | tf_op jit(solution)/shard_map/ppermute | solution.py:75
  3.3 8.1 %collective-permute-start.1 = (bf16[1,256,256]{2,1,0:T(8,128)(2,1)S(1)}, bf16[1,256,256]{2,1,0:T(8,128)(2,1)S(1)}, u32[]{:S(2)}, u32[]{:S(2)}) collective-permute-start(bf16[1,256,256]{2,1,0:T(8,128)(2,1)S(1)} %bitcast.126), channel_id=1, source_target_pairs={{0,16},{2,18},{4,20},{6,22},{8,24},{10,26},{12,28},{14,30},{16,0},... | collective-permute-start | bytes 393224 | tf_op jit(solution)/shard_map/ppermute | solution.py:75
  6.0 11.3 %collective-permute-start.2 = (bf16[1,256,256]{2,1,0:T(8,128)(2,1)S(1)}, bf16[1,256,256]{2,1,0:T(8,128)(2,1)S(1)}, u32[]{:S(2)}, u32[]{:S(2)}) collective-permute-start(bf16[1,256,256]{2,1,0:T(8,128)(2,1)S(1)} %bitcast.127), channel_id=1, source_target_pairs={{0,24},{2,26},{4,28},{6,30},{8,16},{10,18},{12,20},{14,22},{16,8},... | collective-permute-start | bytes 393224 | tf_op jit(solution)/shard_map/ppermute | solution.py:75
  6.2 97.6 %collective-permute-start.9 = (bf16[512,2048]{1,0:T(8,128)(2,1)}, bf16[512,2048]{1,0:T(8,128)(2,1)}, u32[]{:S(2)}, u32[]{:S(2)}) collective-permute-start(bf16[512,2048]{1,0:T(8,128)(2,1)} %param.18), channel_id=1, source_target_pairs={{0,1},{1,0},{2,3},{3,2},{4,5},{5,4},{6,7},{7,6},{8,9},{9,8},{10,11... | collective-permute-start | bytes 6291464 | tf_op jit(solution)/shard_map/ppermute | solution.py:75
  18.0 6.1 %collective-permute-start.3 = (bf16[1,1,1024,128]{3,2,1,0:T(8,128)(2,1)S(1)}, bf16[1,1,1024,128]{3,2,1,0:T(8,128)(2,1)S(1)}, u32[]{:S(2)}, u32[]{:S(2)}) collective-permute-start(bf16[1,1,1024,128]{3,2,1,0:T(8,128)(2,1)S(1)} %get-tuple-element.24), channel_id=1, source_target_pairs={{0,2},{2,0},{4,6},{6,4},{8,10},{10,8},{12,14},{14,12},{16,18},{18,... | collective-permute-start | bytes 786440 | tf_op jit(solution)/shard_map/ppermute | solution.py:75
  19.3 7.1 %collective-permute-start.10 = (bf16[128,1024]{1,0:T(8,128)(2,1)S(1)}, bf16[128,1024]{1,0:T(8,128)(2,1)S(1)}, u32[]{:S(2)}, u32[]{:S(2)}) collective-permute-start(bf16[128,1024]{1,0:T(8,128)(2,1)S(1)} %get-tuple-element.13), channel_id=1, source_target_pairs={{0,8},{2,10},{4,12},{6,14},{8,0},{10,2},{12,4},{14,6},{16,24},{18,... | collective-permute-start | bytes 786440 | tf_op jit(solution)/shard_map/ppermute | solution.py:75
  19.4 12.8 %collective-permute-start.11 = (bf16[128,1024]{1,0:T(8,128)(2,1)S(1)}, bf16[128,1024]{1,0:T(8,128)(2,1)S(1)}, u32[]{:S(2)}, u32[]{:S(2)}) collective-permute-start(bf16[128,1024]{1,0:T(8,128)(2,1)S(1)} %get-tuple-element.15), channel_id=1, source_target_pairs={{0,16},{2,18},{4,20},{6,22},{8,24},{10,26},{12,28},{14,30},{16,0},... | collective-permute-start | bytes 786440 | tf_op jit(solution)/shard_map/ppermute | solution.py:75
  22.0 22.3 %collective-permute-start.12 = (bf16[128,1024]{1,0:T(8,128)(2,1)S(1)}, bf16[128,1024]{1,0:T(8,128)(2,1)S(1)}, u32[]{:S(2)}, u32[]{:S(2)}) collective-permute-start(bf16[128,1024]{1,0:T(8,128)(2,1)S(1)} %get-tuple-element.14), channel_id=1, source_target_pairs={{0,24},{2,26},{4,28},{6,30},{8,16},{10,18},{12,20},{14,22},{16,8},... | collective-permute-start | bytes 786440 | tf_op jit(solution)/shard_map/ppermute | solution.py:75
  24.2 22.8 %copy-start.12 = (bf16[1,1,1024,128]{3,2,1,0:T(8,128)(2,1)}, bf16[1,1,1024,128]{3,2,1,0:T(8,128)(2,1)S(1)}, u32[]{:S(2)}) copy-start(bf16[1,1,1024,128]{3,2,1,0:T(8,128)(2,1)S(1)} %collective-permute-done.3) | copy-start | bytes 786436
  24.2 23.0 %collective-permute-start.15 = (bf16[1024,128]{1,0:T(8,128)(2,1)S(1)}, bf16[1024,128]{1,0:T(8,128)(2,1)S(1)}, u32[]{:S(2)}, u32[]{:S(2)}) collective-permute-start(bf16[1024,128]{1,0:T(8,128)(2,1)S(1)} %get-tuple-element.17), channel_id=1, source_target_pairs={{0,8},{2,10},{4,12},{6,14},{8,0},{10,2},{12,4},{14,6},{16,24},{18,... | collective-permute-start | bytes 786440 | tf_op jit(solution)/shard_map/ppermute | solution.py:75
  26.5 40.6 %collective-permute-start.4 = (bf16[2,1,1024,128]{3,2,1,0:T(8,128)(2,1)}, bf16[2,1,1024,128]{3,2,1,0:T(8,128)(2,1)}, u32[]{:S(2)}, u32[]{:S(2)}) collective-permute-start(bf16[2,1,1024,128]{3,2,1,0:T(8,128)(2,1)} %pad_maximum_fusion.6), channel_id=1, source_target_pairs={{0,4},{2,6},{4,0},{6,2},{8,12},{10,14},{12,8},{14,10},{16,20},{18,... | collective-permute-start | bytes 1572872 | tf_op jit(solution)/shard_map/ppermute | solution.py:75
  32.3 27.6 %collective-permute-start.16 = (bf16[1024,128]{1,0:T(8,128)(2,1)S(1)}, bf16[1024,128]{1,0:T(8,128)(2,1)S(1)}, u32[]{:S(2)}, u32[]{:S(2)}) collective-permute-start(bf16[1024,128]{1,0:T(8,128)(2,1)S(1)} %get-tuple-element.19), channel_id=1, source_target_pairs={{0,16},{2,18},{4,20},{6,22},{8,24},{10,26},{12,28},{14,30},{16,0},... | collective-permute-start | bytes 786440 | tf_op jit(solution)/shard_map/ppermute | solution.py:75
  44.3 21.3 %collective-permute-start.17 = (bf16[1024,128]{1,0:T(8,128)(2,1)S(1)}, bf16[1024,128]{1,0:T(8,128)(2,1)S(1)}, u32[]{:S(2)}, u32[]{:S(2)}) collective-permute-start(bf16[1024,128]{1,0:T(8,128)(2,1)S(1)} %get-tuple-element.18), channel_id=1, source_target_pairs={{0,24},{2,26},{4,28},{6,30},{8,16},{10,18},{12,20},{14,22},{16,8},... | collective-permute-start | bytes 786440 | tf_op jit(solution)/shard_map/ppermute | solution.py:75
  47.1 51.7 %collective-permute-start.13 = (bf16[1,4,128,1024]{3,2,1,0:T(8,128)(2,1)S(1)}, bf16[1,4,128,1024]{3,2,1,0:T(8,128)(2,1)S(1)}, u32[]{:S(2)}, u32[]{:S(2)}) collective-permute-start(bf16[1,4,128,1024]{3,2,1,0:T(8,128)(2,1)S(1)} %maximum_bitcast_fusion), channel_id=1, source_target_pairs={{0,2},{2,0},{4,6},{6,4},{8,10},{10,8},{12,14},{14,12},{16,18},{18,... | collective-permute-start | bytes 3145736 | tf_op jit(solution)/shard_map/ppermute | solution.py:75
  65.8 35.0 %collective-permute-start.18 = (bf16[1,4,1024,128]{3,2,1,0:T(8,128)(2,1)S(1)}, bf16[1,4,1024,128]{3,2,1,0:T(8,128)(2,1)}, u32[]{:S(2)}, u32[]{:S(2)}) collective-permute-start(bf16[1,4,1024,128]{3,2,1,0:T(8,128)(2,1)S(1)} %maximum_bitcast_fusion.1), channel_id=1, source_target_pairs={{0,4},{2,6},{4,0},{6,2},{8,12},{10,14},{12,8},{14,10},{16,20},{18,... | collective-permute-start | bytes 3145736 | tf_op jit(solution)/shard_map/ppermute | solution.py:75
  85.8 3.7 %collective-permute-start.5 = (bf16[256,128]{1,0:T(8,128)(2,1)}, bf16[256,128]{1,0:T(8,128)(2,1)}, u32[]{:S(2)}, u32[]{:S(2)}) collective-permute-start(bf16[256,128]{1,0:T(8,128)(2,1)} %get-tuple-element.34), channel_id=1, source_target_pairs={{0,8},{2,10},{4,12},{6,14},{8,0},{10,2},{12,4},{14,6},{16,24},{18,... | collective-permute-start | bytes 196616 | tf_op jit(solution)/shard_map/ppermute | solution.py:75
  85.8 6.6 %collective-permute-start.6 = (bf16[256,128]{1,0:T(8,128)(2,1)S(1)}, bf16[256,128]{1,0:T(8,128)(2,1)S(1)}, u32[]{:S(2)}, u32[]{:S(2)}) collective-permute-start(bf16[256,128]{1,0:T(8,128)(2,1)S(1)} %get-tuple-element.33), channel_id=1, source_target_pairs={{0,16},{2,18},{4,20},{6,22},{8,24},{10,26},{12,28},{14,30},{16,0},... | collective-permute-start | bytes 196616 | tf_op jit(solution)/shard_map/ppermute | solution.py:75
  89.5 4.8 %collective-permute-start.7 = (bf16[256,128]{1,0:T(8,128)(2,1)S(1)}, bf16[256,128]{1,0:T(8,128)(2,1)S(1)}, u32[]{:S(2)}, u32[]{:S(2)}) collective-permute-start(bf16[256,128]{1,0:T(8,128)(2,1)S(1)} %get-tuple-element.32), channel_id=1, source_target_pairs={{0,24},{2,26},{4,28},{6,30},{8,16},{10,18},{12,20},{14,22},{16,8},... | collective-permute-start | bytes 196616 | tf_op jit(solution)/shard_map/ppermute | solution.py:75
  94.3 9.5 %collective-permute-start.8 = (bf16[256,512]{1,0:T(8,128)(2,1)S(1)}, bf16[256,512]{1,0:T(8,128)(2,1)S(1)}, u32[]{:S(2)}, u32[]{:S(2)}) collective-permute-start(bf16[256,512]{1,0:T(8,128)(2,1)S(1)} %constant_dynamic-update-slice_fusion.11), channel_id=1, source_target_pairs={{0,1},{1,0},{2,3},{3,2},{4,5},{5,4},{6,7},{7,6},{8,9},{9,8},{10,11... | collective-permute-start | bytes 786440 | tf_op jit(solution)/shard_map/ppermute | solution.py:75
  98.8 4.7 %copy-start = (bf16[1,4,128,1024]{3,2,1,0:T(8,128)(2,1)}, bf16[1,4,128,1024]{3,2,1,0:T(8,128)(2,1)S(1)}, u32[]{:S(2)}) copy-start(bf16[1,4,128,1024]{3,2,1,0:T(8,128)(2,1)S(1)} %collective-permute-done.13) | copy-start | bytes 3145732
  100.5 5.6 %copy-start.10 = (bf16[256,2048]{1,0:T(8,128)(2,1)S(1)}, bf16[256,2048]{1,0:T(8,128)(2,1)}, u32[]{:S(2)}) copy-start(bf16[256,2048]{1,0:T(8,128)(2,1)} %param.19) | copy-start | bytes 3145732
  100.5 67.9 %collective-permute-start.14 = (bf16[2,4,128,1024]{3,2,1,0:T(8,128)(2,1)}, bf16[2,4,128,1024]{3,2,1,0:T(8,128)(2,1)}, u32[]{:S(2)}, u32[]{:S(2)}) collective-permute-start(bf16[2,4,128,1024]{3,2,1,0:T(8,128)(2,1)} %pad_maximum_fusion.2), channel_id=1, source_target_pairs={{0,4},{2,6},{4,0},{6,2},{8,12},{10,14},{12,8},{14,10},{16,20},{18,... | collective-permute-start | bytes 6291464 | tf_op jit(solution)/shard_map/ppermute | solution.py:75
  103.6 66.6 %collective-permute-start.19 = (bf16[2,4,1024,128]{3,2,1,0:T(8,128)(2,1)}, bf16[2,4,1024,128]{3,2,1,0:T(8,128)(2,1)}, u32[]{:S(2)}, u32[]{:S(2)}) collective-permute-start(bf16[2,4,1024,128]{3,2,1,0:T(8,128)(2,1)} %pad_maximum_fusion.3), channel_id=1, source_target_pairs={{0,2},{2,0},{4,6},{6,4},{8,10},{10,8},{12,14},{14,12},{16,18},{18,... | collective-permute-start | bytes 6291464 | tf_op jit(solution)/shard_map/ppermute | solution.py:75
  106.2 3.0 %copy-start.16 = (f32[2048]{0:T(1024)S(1)}, f32[2048]{0:T(1024)}, u32[]{:S(2)}) copy-start(f32[2048]{0:T(1024)} %param.21) | copy-start | bytes 24580
  106.2 3.0 %copy-start.17 = (f32[2048]{0:T(1024)S(1)}, f32[2048]{0:T(1024)}, u32[]{:S(2)}) copy-start(f32[2048]{0:T(1024)} %param.20) | copy-start | bytes 24580
  110.4 22.5 %collective-permute-start.21 = (bf16[256,1024]{1,0:T(8,128)(2,1)}, bf16[256,1024]{1,0:T(8,128)(2,1)}, u32[]{:S(2)}, u32[]{:S(2)}) collective-permute-start(bf16[256,1024]{1,0:T(8,128)(2,1)} %constant_dynamic-slice_fusion.10), channel_id=1, source_target_pairs={{0,8},{2,10},{4,12},{6,14},{8,0},{10,2},{12,4},{14,6},{16,24},{18,... | collective-permute-start | bytes 1572872 | tf_op jit(solution)/shard_map/ppermute | solution.py:75
  111.4 24.8 %collective-permute-start.25 = (bf16[256,1024]{1,0:T(8,128)(2,1)}, bf16[256,1024]{1,0:T(8,128)(2,1)}, u32[]{:S(2)}, u32[]{:S(2)}) collective-permute-start(bf16[256,1024]{1,0:T(8,128)(2,1)} %constant_dynamic-slice_fusion.10), channel_id=1, source_target_pairs={{0,16},{2,18},{4,20},{6,22},{8,24},{10,26},{12,28},{14,30},{16,0},... | collective-permute-start | bytes 1572872 | tf_op jit(solution)/shard_map/ppermute | solution.py:75
  112.8 45.7 %collective-permute-start.29 = (bf16[256,1024]{1,0:T(8,128)(2,1)}, bf16[256,1024]{1,0:T(8,128)(2,1)}, u32[]{:S(2)}, u32[]{:S(2)}) collective-permute-start(bf16[256,1024]{1,0:T(8,128)(2,1)} %constant_dynamic-slice_fusion.10), channel_id=1, source_target_pairs={{0,24},{2,26},{4,28},{6,30},{8,16},{10,18},{12,20},{14,22},{16,8},... | collective-permute-start | bytes 1572872 | tf_op jit(solution)/shard_map/ppermute | solution.py:75
  133.0 30.8 %collective-permute-start.22 = (bf16[256,1024]{1,0:T(8,128)(2,1)}, bf16[256,1024]{1,0:T(8,128)(2,1)}, u32[]{:S(2)}, u32[]{:S(2)}) collective-permute-start(bf16[256,1024]{1,0:T(8,128)(2,1)} %collective-permute-done.21), channel_id=1, source_target_pairs={{0,1},{1,0},{2,3},{3,2},{4,5},{5,4},{6,7},{7,6},{8,9},{9,8},{10,11... | collective-permute-start | bytes 1572872 | tf_op jit(solution)/shard_map/ppermute | solution.py:75
  136.2 28.8 %collective-permute-start.26 = (bf16[256,1024]{1,0:T(8,128)(2,1)}, bf16[256,1024]{1,0:T(8,128)(2,1)}, u32[]{:S(2)}, u32[]{:S(2)}) collective-permute-start(bf16[256,1024]{1,0:T(8,128)(2,1)} %collective-permute-done.25), channel_id=1, source_target_pairs={{0,1},{1,0},{2,3},{3,2},{4,5},{5,4},{6,7},{7,6},{8,9},{9,8},{10,11... | collective-permute-start | bytes 1572872 | tf_op jit(solution)/shard_map/ppermute | solution.py:75
  158.5 7.9 %collective-permute-start.30 = (bf16[256,1024]{1,0:T(8,128)(2,1)}, bf16[256,1024]{1,0:T(8,128)(2,1)S(1)}, u32[]{:S(2)}, u32[]{:S(2)}) collective-permute-start(bf16[256,1024]{1,0:T(8,128)(2,1)} %collective-permute-done.29), channel_id=1, source_target_pairs={{0,1},{1,0},{2,3},{3,2},{4,5},{5,4},{6,7},{7,6},{8,9},{9,8},{10,11... | collective-permute-start | bytes 1572872 | tf_op jit(solution)/shard_map/ppermute | solution.py:75
  160.2 8.2 %copy-start.1 = (bf16[1,4,128,1024]{3,2,1,0:T(8,128)(2,1)S(1)}, bf16[1,4,128,1024]{3,2,1,0:T(8,128)(2,1)}, u32[]{:S(2)}) copy-start(bf16[1,4,128,1024]{3,2,1,0:T(8,128)(2,1)} %copy-done) | copy-start | bytes 3145732
  188.3 6.9 %copy-start.7 = (bf16[256,2048]{1,0:T(8,128)(2,1)S(1)}, bf16[256,2048]{1,0:T(8,128)(2,1)}, u32[]{:S(2)}) copy-start(bf16[256,2048]{1,0:T(8,128)(2,1)} %copy-done.6) | copy-start | bytes 3145732
  195.2 8.7 %copy-start.9 = (bf16[256,2048]{1,0:T(8,128)(2,1)S(1)}, bf16[256,2048]{1,0:T(8,128)(2,1)}, u32[]{:S(2)}) copy-start(bf16[256,2048]{1,0:T(8,128)(2,1)} %copy-done.8) | copy-start | bytes 3145732
  204.0 9.2 %copy-start.5 = (bf16[256,2048]{1,0:T(8,128)(2,1)S(1)}, bf16[256,2048]{1,0:T(8,128)(2,1)}, u32[]{:S(2)}) copy-start(bf16[256,2048]{1,0:T(8,128)(2,1)} %copy-done.4) | copy-start | bytes 3145732
  204.0 16.8 %collective-permute-start.23 = (bf16[256,1024]{1,0:T(8,128)(2,1)}, bf16[256,1024]{1,0:T(8,128)(2,1)}, u32[]{:S(2)}, u32[]{:S(2)}) collective-permute-start(bf16[256,1024]{1,0:T(8,128)(2,1)} %constant_dynamic-slice_fusion.2), channel_id=1, source_target_pairs={{0,1},{1,0},{2,3},{3,2},{4,5},{5,4},{6,7},{7,6},{8,9},{9,8},{10,11... | collective-permute-start | bytes 1572872 | tf_op jit(solution)/shard_map/ppermute | solution.py:75
  212.7 9.5 %collective-permute-start.27 = (bf16[256,1024]{1,0:T(8,128)(2,1)}, bf16[256,1024]{1,0:T(8,128)(2,1)}, u32[]{:S(2)}, u32[]{:S(2)}) collective-permute-start(bf16[256,1024]{1,0:T(8,128)(2,1)} %constant_dynamic-slice_fusion.1), channel_id=1, source_target_pairs={{0,1},{1,0},{2,3},{3,2},{4,5},{5,4},{6,7},{7,6},{8,9},{9,8},{10,11... | collective-permute-start | bytes 1572872 | tf_op jit(solution)/shard_map/ppermute | solution.py:75
  219.0 52.7 %copy-start.11 = (bf16[256,2048]{1,0:T(8,128)(2,1)S(1)}, bf16[256,2048]{1,0:T(8,128)(2,1)}, u32[]{:S(2)}) copy-start(bf16[256,2048]{1,0:T(8,128)(2,1)} %convolution_convert_fusion.5) | copy-start | bytes 3145732
  219.0 7.0 %collective-permute-start.31 = (bf16[256,1024]{1,0:T(8,128)(2,1)S(1)}, bf16[256,1024]{1,0:T(8,128)(2,1)S(1)}, u32[]{:S(2)}, u32[]{:S(2)}) collective-permute-start(bf16[256,1024]{1,0:T(8,128)(2,1)S(1)} %constant_dynamic-slice_fusion), channel_id=1, source_target_pairs={{0,1},{1,0},{2,3},{3,2},{4,5},{5,4},{6,7},{7,6},{8,9},{9,8},{10,11... | collective-permute-start | bytes 1572872 | tf_op jit(solution)/shard_map/ppermute | solution.py:75
  220.4 55.4 %dynamic-slice-start = ((f32[2048]{0:T(1024)}, s32[]{:T(128)}), f32[1024]{0:T(1024)S(1)}, s32[]{:S(2)}) async-start(f32[2048]{0:T(1024)} %param.24, s32[]{:T(128)} %select_n.385), calls=%async_computation | async-start | bytes 8704 | tf_op jit(solution)/shard_map/dynamic_slice | solution.py:70
  220.4 55.3 %dynamic-slice-start.1 = ((f32[2048]{0:T(1024)}, s32[]{:T(128)}), f32[1024]{0:T(1024)S(1)}, s32[]{:S(2)}) async-start(f32[2048]{0:T(1024)} %param.25, s32[]{:T(128)} %select_n.385), calls=%async_computation.1 | async-start | bytes 8704 | tf_op jit(solution)/shard_map/dynamic_slice | solution.py:70
  220.4 6.2 %collective-permute-start.20 = (bf16[256,1024]{1,0:T(8,128)(2,1)S(1)}, bf16[256,1024]{1,0:T(8,128)(2,1)S(1)}, u32[]{:S(2)}, u32[]{:S(2)}) collective-permute-start(bf16[256,1024]{1,0:T(8,128)(2,1)S(1)} %constant_dynamic-slice_fusion.3), channel_id=1, source_target_pairs={{0,1},{1,0},{2,3},{3,2},{4,5},{5,4},{6,7},{7,6},{8,9},{9,8},{10,11... | collective-permute-start | bytes 1572872 | tf_op jit(solution)/shard_map/ppermute | solution.py:75
  222.2 20.9 %collective-permute-start.24 = (bf16[256,1024]{1,0:T(8,128)(2,1)S(1)}, bf16[256,1024]{1,0:T(8,128)(2,1)S(1)}, u32[]{:S(2)}, u32[]{:S(2)}) collective-permute-start(bf16[256,1024]{1,0:T(8,128)(2,1)S(1)} %add_convert_fusion.4), channel_id=1, source_target_pairs={{0,8},{2,10},{4,12},{6,14},{8,0},{10,2},{12,4},{14,6},{16,24},{18,... | collective-permute-start | bytes 1572872 | tf_op jit(solution)/shard_map/ppermute | solution.py:75
  223.7 35.7 %collective-permute-start.28 = (bf16[256,1024]{1,0:T(8,128)(2,1)S(1)}, bf16[256,1024]{1,0:T(8,128)(2,1)S(1)}, u32[]{:S(2)}, u32[]{:S(2)}) collective-permute-start(bf16[256,1024]{1,0:T(8,128)(2,1)S(1)} %add_convert_fusion.3), channel_id=1, source_target_pairs={{0,16},{2,18},{4,20},{6,22},{8,24},{10,26},{12,28},{14,30},{16,0},... | collective-permute-start | bytes 1572872 | tf_op jit(solution)/shard_map/ppermute | solution.py:75
  226.2 45.5 %collective-permute-start.32 = (bf16[256,1024]{1,0:T(8,128)(2,1)S(1)}, bf16[256,1024]{1,0:T(8,128)(2,1)S(1)}, u32[]{:S(2)}, u32[]{:S(2)}) collective-permute-start(bf16[256,1024]{1,0:T(8,128)(2,1)S(1)} %add_convert_fusion.2), channel_id=1, source_target_pairs={{0,24},{2,26},{4,28},{6,30},{8,16},{10,18},{12,20},{14,22},{16,8},... | collective-permute-start | bytes 1572872 | tf_op jit(solution)/shard_map/ppermute | solution.py:75
  (6 other events, 10.7 us)

commit v2 on v1

--- a/solution.py
+++ b/solution.py
@@ -79,11 +79,47 @@
     bits = [1 << b for b in range(low_count.bit_length() - 1)]
     slots = {0: array_in}
     for bit in bits if ascending else bits[::-1]:
-        order = sorted(slots)
-        got = swap(jnp.stack([slots[e] for e in order], 0), "sp", bit)
-        for n, e in enumerate(order):
-            slots[e ^ bit] = got[n]
-    return jnp.stack([slots[e] for e in range(low_count)], 0)
+        for e in sorted(slots):
+            slots[e ^ bit] = swap(slots[e], "sp", bit)
+    return [slots[e] for e in range(low_count)]
+
+
+def place_blocks(pieces, me, core, n_tp, axis):
+    low_count = len(pieces)
+    split, rows, cols = pieces[0].shape
+    n_sp = low_count * split
+    width = (rows, cols)[axis]
+    part = n_sp * width // n_tp
+    out_shape = (n_sp * rows, cols) if axis == 0 else (rows, n_sp * cols)
+    starts = []
+    for e in range(low_count):
+        for d in range(split):
+            at = (me ^ (d * low_count + e)) * width
+            starts.append(((at // part) ^ core) * part + at % part)
+
+    if width % 128:
+        out = jnp.zeros(out_shape, jnp.bfloat16)
+        for n, at in enumerate(starts):
+            out = lax.dynamic_update_slice_in_dim(out, pieces[n // split][n % split], at, axis)
+        return out
+
+    def kernel(starts_ref, *refs):
+        o_ref = refs[-1]
+        for e in range(low_count):
+            for d in range(split):
+                at = pl.multiple_of(starts_ref[e * split + d], 128)
+                if axis == 0:
+                    o_ref[pl.ds(at, rows), :] = refs[e][d]
+                else:
+                    o_ref[:, pl.ds(at, cols)] = refs[e][d]
+
+    return pl.pallas_call(
+        kernel,
+        in_specs=[pl.BlockSpec(memory_space=pltpu.SMEM)]
+        + [pl.BlockSpec(memory_space=pltpu.VMEM)] * low_count,
+        out_specs=pl.BlockSpec(memory_space=pltpu.VMEM),
+        out_shape=jax.ShapeDtypeStruct(out_shape, jnp.bfloat16),
+    )(jnp.stack(starts).astype(jnp.int32), *pieces)
 
 
 def attend_kernel(q_ref, kv_ref, o_ref):
@@ -165,7 +201,7 @@
             block = lax.dynamic_slice_in_dim(packed, (hi ^ d) * per, per, 0)
             parts.append(block if d == 0 else swap(block, "sp", d * low_count))
         got = jnp.concatenate(parts, 1)
-        kv_all = gather_low(got[..., q_width:], low_count)
+        kv_all = jnp.stack(gather_low(got[..., q_width:], low_count), 0)
         heads_out = []
         for h in range(per):
             kv_rows = kv_all[:, h].reshape(-1, 2 * HEAD_SIZE)
@@ -197,21 +233,8 @@
         down_parts.append(down_block)
     up_all = gather_low(jnp.stack(up_parts, 0), low_count)
     down_all = gather_low(jnp.stack(down_parts, 0), low_count, ascending=False)
-
-    def placed(pieces, axis):
-        ordered = []
-        for s in range(n_sp):
-            rel = me ^ s
-            piece = lax.dynamic_slice(
-                pieces,
-                (rel % low_count, rel // low_count, 0, 0),
-                (1, 1) + pieces.shape[2:],
-            )
-            ordered.append(piece.reshape(pieces.shape[2:]))
-        return jnp.concatenate(ordered, axis)
-
-    up_own = placed(up_all, 0)
-    down_own = placed(down_all, 1)
+    up_own = place_blocks(up_all, me, core, n_tp, 0)
+    down_own = place_blocks(down_all, me, core, n_tp, 1)
 
     mixed_sum = jnp.zeros((tok_rows, D), jnp.float32)
     for d in range(n_tp):
@@ -227,17 +250,15 @@
     normed_own = take_cols(full_rows, core * col_width, col_width)
 
     ffn_cols = jnp.zeros((tok_rows, col_width), jnp.float32)
-    for d in range(split):
+    for d in [*range(1, split), 0]:
         if d == 0:
-            rows_d = full_rows
+            pieces = [
+                take_cols(full_rows, (core ^ e) * col_width, col_width) for e in range(n_tp)
+            ]
         else:
             mine = swap(normed_own, "sp", d * low_count)
-            rows_d = jnp.zeros((tok_rows, D), jnp.bfloat16)
-            for e in range(n_tp):
-                piece = mine if e == 0 else swap(mine, "tp", e)
-                rows_d = lax.dynamic_update_slice_in_dim(
-                    rows_d, piece, (core ^ e) * col_width, 1
-                )
+            pieces = [mine] + [swap(mine, "tp", e) for e in range(1, n_tp)]
+        rows_d = jnp.concatenate(pieces, 1)
         up_acts = jnp.dot(rows_d, up_own, preferred_element_type=jnp.float32)
         hidden = jnp.square(jnp.maximum(up_acts, 0.0)).astype(jnp.bfloat16)
         partial_ffn = jnp.dot(hidden, down_own, preferred_element_type=jnp.float32).astype(
@@ -245,7 +266,7 @@
         )
         cols = jnp.zeros((tok_rows, col_width), jnp.float32)
         for e in range(n_tp):
-            piece = take_cols(partial_ffn, (core ^ e) * col_width, col_width)
+            piece = partial_ffn[:, e * col_width : (e + 1) * col_width]
             if e:
                 piece = swap(piece, "tp", e)
             cols = cols + piece.astype(jnp.float32)

time: 278 us -> 246 us (0.88)
  local copies, waits for them, and re-layouts: 35.6 us -> 9.75 us
  waiting for transfers between devices: 127 us -> 108 us
  starting transfers between devices: 45.9 us -> 57 us
  Pallas kernels: 14.9 us -> 24.8 us
  other arithmetic: 18.3 us -> 10.8 us
  matrix products: 31.3 us -> 28.2 us
    ppermute x33 -> x36, waiting for transfers between devices: 127 us -> 108 us  [swap(): lax.ppermute(array_in, axis_name, [(i, i ^ offset) for i in range(size)])]
    unnamed x72 -> x32, local copies, waits for them, and re-layouts: 17.1 us -> 1.87 us
    ppermute x33 -> x36, starting transfers between devices: 45.9 us -> 57 us  [swap(): lax.ppermute(array_in, axis_name, [(i, i ^ offset) for i in range(size)])]
    pallas_call x0 -> x2, Pallas kernels: none -> 9.85 us  [place_blocks(): pl.pallas_call(kernel, in_specs=[pl.BlockSpec(memory_space=pltpu.SMEM)] +...]
    another operation x8 -> x3, other arithmetic: 11.4 us -> 3.34 us  [the longest x1 2.13 us: local(): kv_all = jnp.stack(gather_low(got[..., q_width:], low_count), 0)]
    dynamic_update_slice x6 -> x0, local copies, waits for them, and re-layouts: 5.93 us -> none  [local(): lax.dynamic_update_slice_in_dim(rows_d, piece, (core ^ e) * col_width, 1)]
    dynamic_slice x9 -> x5, local copies, waits for them, and re-layouts: 5.83 us -> 0.09 us  [take_cols(): lax.dynamic_slice_in_dim(array_in, col_start, col_width, array_in.ndim - 1)]
  transfers between devices with their start and end apart: 33 -> 36, of which waited for: 16 -> 13; matrix products, arithmetic and copies ran while one was open for 16% -> 18% of each run, Pallas kernels for 5% -> 10%
where the time goes in v2:
time: 246 us; the launch traced here: 242 us
  waiting for transfers between devices  108 us (44%)
  starting transfers between devices  57 us (23%)
  matrix products  28.2 us (11%)
  Pallas kernels  24.8 us (10%)
  other arithmetic  10.8 us (4%)
  local copies, waits for them, and re-layouts  9.75 us (4%)
  blocking collectives  3.25 us (1%)
    ppermute x36, waiting for transfers between devices, swap(): lax.ppermute(array_in, axis_name, [(i, i ^ offset) for i in range(size)])  108 us
    ppermute x36, starting transfers between devices, swap(): lax.ppermute(array_in, axis_name, [(i, i ^ offset) for i in range(size)])  57 us
    dot_general x4, matrix products, local(): jnp.dot(hidden, down_own, preferred_element_type=jnp.float32)  24.9 us
    pallas_call x1, Pallas kernels, attend(): pl.pallas_call(attend_kernel, grid=(rows // block,), in_specs=[pl.BlockSp...  14.9 us
    pallas_call x2, Pallas kernels, place_blocks(): pl.pallas_call(kernel, in_specs=[pl.BlockSpec(memory_space=pltpu.SMEM)] +...  9.85 us
  transfers between devices with their start and end apart: 36, of which 13 were waited for; matrix products, arithmetic and copies ran while one was open for 18% of the time, Pallas kernels for 10%

profile of v2, /device:TPU:9, one launch (start us, length us, event | category | flops | bytes accessed | tf_op | source)
XLA Modules:
  0.0 242.3 jit_solution(7089721970970164433)
XLA Ops:
  0.0 1.1 copy.16
  3.3 1.4 collective-permute-start.2
  4.7 1.1 collective-permute-start.1
  5.9 1.2 collective-permute-start
  7.2 1.2 collective-permute-start.10
  9.3 1.2 collective-permute-start.21
  10.8 2.9 %collective-permute-done.2 = bf16[1,256,256]{2,1,0:T(8,128)(2,1)} collective-permute-done((bf16[1,256,256]{2,1,0:T(8,128)(2,1)S(1)}, bf16[1,256,256]{2,1,0:T(8,128)(2,1)}, u32[]{:S(2)}, u32[]{:S(2)}) %collective-permute-start.2) | collective-permute-done | bytes 131104 | tf_op jit(solution)/shard_map/ppermute | solution.py:75
  13.6 1.9 collective-permute-done.1
  15.6 13.3 %collective-permute-start.19 = (bf16[1024,128]{1,0:T(8,128)(2,1)S(1)}, bf16[1024,128]{1,0:T(8,128)(2,1)S(1)}, u32[]{:S(2)}, u32[]{:S(2)}) collective-permute-start(bf16[1024,128]{1,0:T(8,128)(2,1)S(1)} %get-tuple-element.17), channel_id=1, source_target_pairs={{0,8},{2,10},{4,12},{6,14},{8,0},{10,2},{12,4},{14,6},{16,24},{18,... | collective-permute-start | bytes 786440 | tf_op jit(solution)/shard_map/ppermute | solution.py:75
  30.7 5.1 %collective-permute-done.21 = bf16[1024,128]{1,0:T(8,128)(2,1)} collective-permute-done((bf16[1024,128]{1,0:T(8,128)(2,1)}, bf16[1024,128]{1,0:T(8,128)(2,1)}, u32[]{:S(2)}, u32[]{:S(2)}) %collective-permute-start.21) | collective-permute-done | bytes 262176 | tf_op jit(solution)/shard_map/ppermute | solution.py:75
  35.8 1.2 collective-permute-start.3
  37.0 6.4 %collective-permute-done.20 = bf16[1024,128]{1,0:T(8,128)(2,1)S(1)} collective-permute-done((bf16[1024,128]{1,0:T(8,128)(2,1)}, bf16[1024,128]{1,0:T(8,128)(2,1)S(1)}, u32[]{:S(2)}, u32[]{:S(2)}) %collective-permute-start.20) | collective-permute-done | bytes 262176 | tf_op jit(solution)/shard_map/ppermute | solution.py:75
  43.4 3.0 %collective-permute-start.14 = (bf16[128,1024]{1,0:T(8,128)(2,1)S(1)}, bf16[128,1024]{1,0:T(8,128)(2,1)S(1)}, u32[]{:S(2)}, u32[]{:S(2)}) collective-permute-start(bf16[128,1024]{1,0:T(8,128)(2,1)S(1)} %get-tuple-element.15), channel_id=1, source_target_pairs={{0,16},{2,18},{4,20},{6,22},{8,24},{10,26},{12,28},{14,30},{16,0},... | collective-permute-start | bytes 786440 | tf_op jit(solution)/shard_map/ppermute | solution.py:75
  46.4 8.7 %collective-permute-done.15 = bf16[128,1024]{1,0:T(8,128)(2,1)S(1)} collective-permute-done((bf16[128,1024]{1,0:T(8,128)(2,1)S(1)}, bf16[128,1024]{1,0:T(8,128)(2,1)S(1)}, u32[]{:S(2)}, u32[]{:S(2)}) %collective-permute-start.15) | collective-permute-done | bytes 262176 | tf_op jit(solution)/shard_map/ppermute | solution.py:75
  55.2 1.2 collective-permute-start.4
  57.7 2.4 %collective-permute-done.14 = bf16[128,1024]{1,0:T(8,128)(2,1)S(1)} collective-permute-done((bf16[128,1024]{1,0:T(8,128)(2,1)S(1)}, bf16[128,1024]{1,0:T(8,128)(2,1)S(1)}, u32[]{:S(2)}, u32[]{:S(2)}) %collective-permute-start.14) | collective-permute-done | bytes 262176 | tf_op jit(solution)/shard_map/ppermute | solution.py:75
  60.2 1.2 collective-permute-start.23
  61.6 1.3 collective-permute-start.16
  62.9 3.0 %collective-permute-done.5 = bf16[1,1024,128]{2,1,0:T(8,128)(2,1)} collective-permute-done((bf16[1,1024,128]{2,1,0:T(8,128)(2,1)}, bf16[1,1024,128]{2,1,0:T(8,128)(2,1)}, u32[]{:S(2)}, u32[]{:S(2)}) %collective-permute-start.5) | collective-permute-done | bytes 262176 | tf_op jit(solution)/shard_map/ppermute | solution.py:75
  65.9 2.1 pad_maximum_fusion
  68.0 14.9 %shard_map.127 = bf16[1024,128]{1,0:T(8,128)(2,1)} custom-call(bf16[1024,128]{1,0:T(8,128)(2,1)} %get-tuple-element.26.q_ref, bf16[4096,128]{1,0:T(8,128)(2,1)} %bitcast.62), custom_call_target="tpu_custom_call" | custom-call | tf_op jit(solution)/shard_map/pallas_call | solution.py:146
  84.0 3.0 %collective-permute-start.7 = (bf16[256,128]{1,0:T(8,128)(2,1)S(1)}, bf16[256,128]{1,0:T(8,128)(2,1)S(1)}, u32[]{:S(2)}, u32[]{:S(2)}) collective-permute-start(bf16[256,128]{1,0:T(8,128)(2,1)S(1)} %get-tuple-element.34), channel_id=1, source_target_pairs={{0,16},{2,18},{4,20},{6,22},{8,24},{10,26},{12,28},{14,30},{16,0},... | collective-permute-start | bytes 196616 | tf_op jit(solution)/shard_map/ppermute | solution.py:75
  87.5 1.8 collective-permute-start.8
  89.4 2.3 collective-permute-done.8
  91.7 8.6 %collective-permute-start.9 = (bf16[256,512]{1,0:T(8,128)(2,1)S(1)}, bf16[256,512]{1,0:T(8,128)(2,1)S(1)}, u32[]{:S(2)}, u32[]{:S(2)}) collective-permute-start(bf16[256,512]{1,0:T(8,128)(2,1)S(1)} %constant_dynamic-update-slice_fusion.1), channel_id=1, source_target_pairs={{0,1},{1,0},{2,3},{3,2},{4,5},{5,4},{6,7},{7,6},{8,9},{9,8},{10,11... | collective-permute-start | bytes 786440 | tf_op jit(solution)/shard_map/ppermute | solution.py:75
  100.3 1.2 collective-permute-start.22
  101.5 1.3 collective-permute-start.17
  102.8 1.2 collective-permute-start.24
  104.1 2.3 fusion.3
  108.7 1.6 collective-permute-start.31
  110.9 14.1 %collective-permute-done.22.refs_1_ = bf16[4,1024,128]{2,1,0:T(8,128)(2,1)} collective-permute-done((bf16[4,1024,128]{2,1,0:T(8,128)(2,1)S(1)}, bf16[4,1024,128]{2,1,0:T(8,128)(2,1)}, u32[]{:S(2)}, u32[]{:S(2)}) %collective-permute-start.22) | collective-permute-done | bytes 1048608 | tf_op jit(solution)/shard_map/ppermute | solution.py:75
  125.0 2.1 collective-permute-start.27
  127.1 20.3 %collective-permute-done.24.refs_3_ = bf16[4,1024,128]{2,1,0:T(8,128)(2,1)} collective-permute-done((bf16[4,1024,128]{2,1,0:T(8,128)(2,1)}, bf16[4,1024,128]{2,1,0:T(8,128)(2,1)}, u32[]{:S(2)}, u32[]{:S(2)}) %collective-permute-start.24) | collective-permute-done | bytes 1048608 | tf_op jit(solution)/shard_map/ppermute | solution.py:75
  148.4 5.4 %shard_map.129 = bf16[1024,2048]{1,0:T(8,128)(2,1)} custom-call(s32[16]{0:T(128)} %stack.134.starts_ref, bf16[4,1024,128]{2,1,0:T(8,128)(2,1)} %copy-done, bf16[4,1024,128]{2,1,0:T(8,128)(2,1)} %collective-permute-done.22.refs_1_, bf16[4,1024,128]{2,1,0:T(8,128)(2,1)} %collective-permute-done.23.refs_2_, bf16[4,1024,128]{2,1,0:T(8,128)(2,1)} %collective-permute-done.24.refs_3_), custom_call_target="tpu_custom_call" | custom-call | tf_op jit(solution)/shard_map/pallas_call | solution.py:116
  153.8 4.5 %shard_map.128 = bf16[2048,1024]{1,0:T(8,128)(2,1)} custom-call(s32[16]{0:T(128)} %stack.134.starts_ref, bf16[4,128,1024]{2,1,0:T(8,128)(2,1)} %copy-done.1, bf16[4,128,1024]{2,1,0:T(8,128)(2,1)} %collective-permute-done.16.refs_1_, bf16[4,128,1024]{2,1,0:T(8,128)(2,1)} %collective-permute-done.17.refs_2_, bf16[4,128,1024]{2,1,0:T(8,128)(2,1)} %collective-permute-done.18.refs_3_), custom_call_target="tpu_custom_call" | custom-call | tf_op jit(solution)/shard_map/pallas_call | solution.py:116
  158.2 1.3 collective-permute-start.32
  159.5 5.8 %convolution_convert_fusion.2 = bf16[256,2048]{1,0:T(8,128)(2,1)S(1)} fusion(bf16[1024,2048]{1,0:T(8,128)(2,1)} %shard_map.129, bf16[2048,1024]{1,0:T(8,128)(2,1)} %shard_map.128, bf16[256,1024]{1,0:T(8,128)(2,1)S(1)} %get-tuple-element.11, bf16[256,1024]{1,0:T(8,128)(2,1)S(1)} %get-tuple-element.10), kind=kOutput, calls=%fused_computation.2 | convolution fusion | flops 2150891520 | bytes 10485760 | tf_op jit(solution)/shard_map/dot_general | solution.py:264
  167.1 6.0 %convolution_convert_fusion.3 = bf16[256,2048]{1,0:T(8,128)(2,1)S(1)} fusion(bf16[1024,2048]{1,0:T(8,128)(2,1)} %shard_map.129, bf16[2048,1024]{1,0:T(8,128)(2,1)} %shard_map.128, bf16[256,1024]{1,0:T(8,128)(2,1)S(1)} %collective-permute-done.32, bf16[256,1024]{1,0:T(8,128)(2,1)} %collective-permute-done.31), kind=kOutput, calls=%fused_computation.3 | convolution fusion | flops 2150891520 | bytes 10485760 | tf_op jit(solution)/shard_map/dot_general | solution.py:264
  174.1 6.1 %convolution_convert_fusion.4 = bf16[256,2048]{1,0:T(8,128)(2,1)S(1)} fusion(bf16[1024,2048]{1,0:T(8,128)(2,1)} %shard_map.129, bf16[2048,1024]{1,0:T(8,128)(2,1)} %shard_map.128, bf16[256,1024]{1,0:T(8,128)(2,1)} %collective-permute-done.28, bf16[256,1024]{1,0:T(8,128)(2,1)} %collective-permute-done.27), kind=kOutput, calls=%fused_computation.4 | convolution fusion | flops 2150891520 | bytes 10485760 | tf_op jit(solution)/shard_map/dot_general | solution.py:264
  181.3 7.1 %convolution_convert_fusion.5 = bf16[256,2048]{1,0:T(8,128)(2,1)} fusion(bf16[1024,2048]{1,0:T(8,128)(2,1)} %shard_map.129, bf16[2048,1024]{1,0:T(8,128)(2,1)} %shard_map.128, bf16[256,1024]{1,0:T(8,128)(2,1)} %collective-permute-done.12, bf16[256,1024]{1,0:T(8,128)(2,1)} %collective-permute-done.11), kind=kOutput, calls=%fused_computation.5 | convolution fusion | flops 2150891520 | bytes 10485760 | tf_op jit(solution)/shard_map/dot_general | solution.py:264
  188.4 1.2 slice.115
  190.1 1.5 collective-permute-start.34
  191.6 1.2 add_convert_fusion.3
  192.9 2.8 %collective-permute-start.30 = (bf16[256,1024]{1,0:T(8,128)(2,1)S(1)}, bf16[256,1024]{1,0:T(8,128)(2,1)S(1)}, u32[]{:S(2)}, u32[]{:S(2)}) collective-permute-start(bf16[256,1024]{1,0:T(8,128)(2,1)S(1)} %add_convert_fusion.3), channel_id=1, source_target_pairs={{0,16},{2,18},{4,20},{6,22},{8,24},{10,26},{12,28},{14,30},{16,0},... | collective-permute-start | bytes 1572872 | tf_op jit(solution)/shard_map/ppermute | solution.py:75
  196.2 29.6 %collective-permute-done.34 = bf16[256,1024]{1,0:T(8,128)(2,1)S(1)} collective-permute-done((bf16[256,1024]{1,0:T(8,128)(2,1)S(1)}, bf16[256,1024]{1,0:T(8,128)(2,1)S(1)}, u32[]{:S(2)}, u32[]{:S(2)}) %collective-permute-start.34) | collective-permute-done | bytes 524320 | tf_op jit(solution)/shard_map/ppermute | solution.py:75
  225.9 10.5 %collective-permute-done.30 = bf16[256,1024]{1,0:T(8,128)(2,1)S(1)} collective-permute-done((bf16[256,1024]{1,0:T(8,128)(2,1)S(1)}, bf16[256,1024]{1,0:T(8,128)(2,1)S(1)}, u32[]{:S(2)}, u32[]{:S(2)}) %collective-permute-start.30) | collective-permute-done | bytes 524320 | tf_op jit(solution)/shard_map/ppermute | solution.py:75
  236.4 1.6 fusion.60
  238.0 3.2 %all-reduce = (f32[256]{0:T(256)S(1)}, f32[256]{0:T(256)S(1)}) all-reduce(f32[256]{0:T(256)S(1)} %get-tuple-element.6, f32[256]{0:T(256)S(1)} %get-tuple-element.5), channel_id=1, replica_groups=mesh['sp'=16,'tp'=2] {'tp'}, use_global_device_ids=true, to_apply=%region_7.8 | all-reduce | flops 512 | bytes 4096 | tf_op jit(solution)/shard_map/psum | solution.py:278
  (119 shorter events, 18.3 us)
Async XLA Ops:
  0.0 2.4 copy-start.9
  2.4 6.0 %copy-start.3 = (bf16[4096,128]{1,0:T(8,128)(2,1)S(1)}, bf16[4096,128]{1,0:T(8,128)(2,1)}, u32[]{:S(2)}) copy-start(bf16[4096,128]{1,0:T(8,128)(2,1)} %param.23) | copy-start | bytes 3145732
  3.1 7.5 %copy-start.4 = (bf16[128,4096]{1,0:T(8,128)(2,1)S(1)}, bf16[128,4096]{1,0:T(8,128)(2,1)}, u32[]{:S(2)}) copy-start(bf16[128,4096]{1,0:T(8,128)(2,1)} %param.22) | copy-start | bytes 3145732
  3.3 10.4 %collective-permute-start.2 = (bf16[1,256,256]{2,1,0:T(8,128)(2,1)S(1)}, bf16[1,256,256]{2,1,0:T(8,128)(2,1)}, u32[]{:S(2)}, u32[]{:S(2)}) collective-permute-start(bf16[1,256,256]{2,1,0:T(8,128)(2,1)S(1)} %bitcast.74), channel_id=1, source_target_pairs={{0,24},{2,26},{4,28},{6,30},{8,16},{10,18},{12,20},{14,22},{16,8},... | collective-permute-start | bytes 393224 | tf_op jit(solution)/shard_map/ppermute | solution.py:75
  4.7 10.8 %collective-permute-start.1 = (bf16[1,256,256]{2,1,0:T(8,128)(2,1)S(1)}, bf16[1,256,256]{2,1,0:T(8,128)(2,1)}, u32[]{:S(2)}, u32[]{:S(2)}) collective-permute-start(bf16[1,256,256]{2,1,0:T(8,128)(2,1)S(1)} %bitcast.73), channel_id=1, source_target_pairs={{0,16},{2,18},{4,20},{6,22},{8,24},{10,26},{12,28},{14,30},{16,0},... | collective-permute-start | bytes 393224 | tf_op jit(solution)/shard_map/ppermute | solution.py:75
  5.9 22.9 %collective-permute-start = (bf16[1,256,256]{2,1,0:T(8,128)(2,1)S(1)}, bf16[1,256,256]{2,1,0:T(8,128)(2,1)S(1)}, u32[]{:S(2)}, u32[]{:S(2)}) collective-permute-start(bf16[1,256,256]{2,1,0:T(8,128)(2,1)S(1)} %bitcast.72), channel_id=1, source_target_pairs={{0,8},{2,10},{4,12},{6,14},{8,0},{10,2},{12,4},{14,6},{16,24},{18,... | collective-permute-start | bytes 393224 | tf_op jit(solution)/shard_map/ppermute | solution.py:75
  7.2 96.9 %collective-permute-start.10 = (bf16[512,2048]{1,0:T(8,128)(2,1)}, bf16[512,2048]{1,0:T(8,128)(2,1)}, u32[]{:S(2)}, u32[]{:S(2)}) collective-permute-start(bf16[512,2048]{1,0:T(8,128)(2,1)} %param.18), channel_id=1, source_target_pairs={{0,1},{1,0},{2,3},{3,2},{4,5},{5,4},{6,7},{7,6},{8,9},{9,8},{10,11... | collective-permute-start | bytes 6291464 | tf_op jit(solution)/shard_map/ppermute | solution.py:75
  9.3 26.5 %collective-permute-start.21 = (bf16[1024,128]{1,0:T(8,128)(2,1)}, bf16[1024,128]{1,0:T(8,128)(2,1)}, u32[]{:S(2)}, u32[]{:S(2)}) collective-permute-start(bf16[1024,128]{1,0:T(8,128)(2,1)} %get-tuple-element.18), channel_id=1, source_target_pairs={{0,24},{2,26},{4,28},{6,30},{8,16},{10,18},{12,20},{14,22},{16,8},... | collective-permute-start | bytes 786440 | tf_op jit(solution)/shard_map/ppermute | solution.py:75
  13.6 29.8 %collective-permute-start.20 = (bf16[1024,128]{1,0:T(8,128)(2,1)}, bf16[1024,128]{1,0:T(8,128)(2,1)S(1)}, u32[]{:S(2)}, u32[]{:S(2)}) collective-permute-start(bf16[1024,128]{1,0:T(8,128)(2,1)} %get-tuple-element.19), channel_id=1, source_target_pairs={{0,16},{2,18},{4,20},{6,22},{8,24},{10,26},{12,28},{14,30},{16,0},... | collective-permute-start | bytes 786440 | tf_op jit(solution)/shard_map/ppermute | solution.py:75
  15.6 30.9 %collective-permute-start.19 = (bf16[1024,128]{1,0:T(8,128)(2,1)S(1)}, bf16[1024,128]{1,0:T(8,128)(2,1)S(1)}, u32[]{:S(2)}, u32[]{:S(2)}) collective-permute-start(bf16[1024,128]{1,0:T(8,128)(2,1)S(1)} %get-tuple-element.17), channel_id=1, source_target_pairs={{0,8},{2,10},{4,12},{6,14},{8,0},{10,2},{12,4},{14,6},{16,24},{18,... | collective-permute-start | bytes 786440 | tf_op jit(solution)/shard_map/ppermute | solution.py:75
  28.9 26.3 %collective-permute-start.15 = (bf16[128,1024]{1,0:T(8,128)(2,1)S(1)}, bf16[128,1024]{1,0:T(8,128)(2,1)S(1)}, u32[]{:S(2)}, u32[]{:S(2)}) collective-permute-start(bf16[128,1024]{1,0:T(8,128)(2,1)S(1)} %get-tuple-element.14), channel_id=1, source_target_pairs={{0,24},{2,26},{4,28},{6,30},{8,16},{10,18},{12,20},{14,22},{16,8},... | collective-permute-start | bytes 786440 | tf_op jit(solution)/shard_map/ppermute | solution.py:75
  35.8 20.6 %collective-permute-start.3 = (bf16[1,1024,128]{2,1,0:T(8,128)(2,1)S(1)}, bf16[1,1024,128]{2,1,0:T(8,128)(2,1)}, u32[]{:S(2)}, u32[]{:S(2)}) collective-permute-start(bf16[1,1024,128]{2,1,0:T(8,128)(2,1)S(1)} %get-tuple-element.25), channel_id=1, source_target_pairs={{0,2},{2,0},{4,6},{6,4},{8,10},{10,8},{12,14},{14,12},{16,18},{18,... | collective-permute-start | bytes 786440 | tf_op jit(solution)/shard_map/ppermute | solution.py:75
  43.4 16.7 %collective-permute-start.14 = (bf16[128,1024]{1,0:T(8,128)(2,1)S(1)}, bf16[128,1024]{1,0:T(8,128)(2,1)S(1)}, u32[]{:S(2)}, u32[]{:S(2)}) collective-permute-start(bf16[128,1024]{1,0:T(8,128)(2,1)S(1)} %get-tuple-element.15), channel_id=1, source_target_pairs={{0,16},{2,18},{4,20},{6,22},{8,24},{10,26},{12,28},{14,30},{16,0},... | collective-permute-start | bytes 786440 | tf_op jit(solution)/shard_map/ppermute | solution.py:75
  46.4 15.0 %collective-permute-start.13 = (bf16[128,1024]{1,0:T(8,128)(2,1)S(1)}, bf16[128,1024]{1,0:T(8,128)(2,1)S(1)}, u32[]{:S(2)}, u32[]{:S(2)}) collective-permute-start(bf16[128,1024]{1,0:T(8,128)(2,1)S(1)} %get-tuple-element.13), channel_id=1, source_target_pairs={{0,8},{2,10},{4,12},{6,14},{8,0},{10,2},{12,4},{14,6},{16,24},{18,... | collective-permute-start | bytes 786440 | tf_op jit(solution)/shard_map/ppermute | solution.py:75
  55.2 7.7 %collective-permute-start.4 = (bf16[1,1024,128]{2,1,0:T(8,128)(2,1)S(1)}, bf16[1,1024,128]{2,1,0:T(8,128)(2,1)S(1)}, u32[]{:S(2)}, u32[]{:S(2)}) collective-permute-start(bf16[1,1024,128]{2,1,0:T(8,128)(2,1)S(1)} %get-tuple-element.25), channel_id=1, source_target_pairs={{0,4},{2,6},{4,0},{6,2},{8,12},{10,14},{12,8},{14,10},{16,20},{18,... | collective-permute-start | bytes 786440 | tf_op jit(solution)/shard_map/ppermute | solution.py:75
  56.4 9.5 %collective-permute-start.5 = (bf16[1,1024,128]{2,1,0:T(8,128)(2,1)}, bf16[1,1024,128]{2,1,0:T(8,128)(2,1)}, u32[]{:S(2)}, u32[]{:S(2)}) collective-permute-start(bf16[1,1024,128]{2,1,0:T(8,128)(2,1)} %collective-permute-done.3), channel_id=1, source_target_pairs={{0,4},{2,6},{4,0},{6,2},{8,12},{10,14},{12,8},{14,10},{16,20},{18,... | collective-permute-start | bytes 786440 | tf_op jit(solution)/shard_map/ppermute | solution.py:75
  57.7 42.5 %copy-start = (bf16[4,1024,128]{2,1,0:T(8,128)(2,1)}, bf16[4,1024,128]{2,1,0:T(8,128)(2,1)S(1)}, u32[]{:S(2)}) copy-start(bf16[4,1024,128]{2,1,0:T(8,128)(2,1)S(1)} %pad_maximum_fusion.2.refs_0_) | copy-start | bytes 3145732
  60.2 42.6 %collective-permute-start.23 = (bf16[4,1024,128]{2,1,0:T(8,128)(2,1)S(1)}, bf16[4,1024,128]{2,1,0:T(8,128)(2,1)}, u32[]{:S(2)}, u32[]{:S(2)}) collective-permute-start(bf16[4,1024,128]{2,1,0:T(8,128)(2,1)S(1)} %pad_maximum_fusion.2.refs_0_), channel_id=1, source_target_pairs={{0,4},{2,6},{4,0},{6,2},{8,12},{10,14},{12,8},{14,10},{16,20},{18,... | collective-permute-start | bytes 3145736 | tf_op jit(solution)/shard_map/ppermute | solution.py:75
  61.6 39.9 %copy-start.1 = (bf16[4,128,1024]{2,1,0:T(8,128)(2,1)}, bf16[4,128,1024]{2,1,0:T(8,128)(2,1)S(1)}, u32[]{:S(2)}) copy-start(bf16[4,128,1024]{2,1,0:T(8,128)(2,1)S(1)} %pad_maximum_fusion.1.refs_0_) | copy-start | bytes 3145732
  61.6 42.3 %collective-permute-start.16 = (bf16[4,128,1024]{2,1,0:T(8,128)(2,1)S(1)}, bf16[4,128,1024]{2,1,0:T(8,128)(2,1)}, u32[]{:S(2)}, u32[]{:S(2)}) collective-permute-start(bf16[4,128,1024]{2,1,0:T(8,128)(2,1)S(1)} %pad_maximum_fusion.1.refs_0_), channel_id=1, source_target_pairs={{0,2},{2,0},{4,6},{6,4},{8,10},{10,8},{12,14},{14,12},{16,18},{18,... | collective-permute-start | bytes 3145736 | tf_op jit(solution)/shard_map/ppermute | solution.py:75
  83.9 3.6 %collective-permute-start.6 = (bf16[256,128]{1,0:T(8,128)(2,1)S(1)}, bf16[256,128]{1,0:T(8,128)(2,1)S(1)}, u32[]{:S(2)}, u32[]{:S(2)}) collective-permute-start(bf16[256,128]{1,0:T(8,128)(2,1)S(1)} %get-tuple-element.35), channel_id=1, source_target_pairs={{0,8},{2,10},{4,12},{6,14},{8,0},{10,2},{12,4},{14,6},{16,24},{18,... | collective-permute-start | bytes 196616 | tf_op jit(solution)/shard_map/ppermute | solution.py:75
  84.0 5.3 %collective-permute-start.7 = (bf16[256,128]{1,0:T(8,128)(2,1)S(1)}, bf16[256,128]{1,0:T(8,128)(2,1)S(1)}, u32[]{:S(2)}, u32[]{:S(2)}) collective-permute-start(bf16[256,128]{1,0:T(8,128)(2,1)S(1)} %get-tuple-element.34), channel_id=1, source_target_pairs={{0,16},{2,18},{4,20},{6,22},{8,24},{10,26},{12,28},{14,30},{16,0},... | collective-permute-start | bytes 196616 | tf_op jit(solution)/shard_map/ppermute | solution.py:75
  87.5 4.2 %collective-permute-start.8 = (bf16[256,128]{1,0:T(8,128)(2,1)S(1)}, bf16[256,128]{1,0:T(8,128)(2,1)S(1)}, u32[]{:S(2)}, u32[]{:S(2)}) collective-permute-start(bf16[256,128]{1,0:T(8,128)(2,1)S(1)} %get-tuple-element.33), channel_id=1, source_target_pairs={{0,24},{2,26},{4,28},{6,30},{8,16},{10,18},{12,20},{14,22},{16,8},... | collective-permute-start | bytes 196616 | tf_op jit(solution)/shard_map/ppermute | solution.py:75
  91.7 9.8 %collective-permute-start.9 = (bf16[256,512]{1,0:T(8,128)(2,1)S(1)}, bf16[256,512]{1,0:T(8,128)(2,1)S(1)}, u32[]{:S(2)}, u32[]{:S(2)}) collective-permute-start(bf16[256,512]{1,0:T(8,128)(2,1)S(1)} %constant_dynamic-update-slice_fusion.1), channel_id=1, source_target_pairs={{0,1},{1,0},{2,3},{3,2},{4,5},{5,4},{6,7},{7,6},{8,9},{9,8},{10,11... | collective-permute-start | bytes 786440 | tf_op jit(solution)/shard_map/ppermute | solution.py:75
  100.3 6.1 %copy-start.2 = (bf16[512,2048]{1,0:T(8,128)(2,1)S(1)}, bf16[512,2048]{1,0:T(8,128)(2,1)}, u32[]{:S(2)}) copy-start(bf16[512,2048]{1,0:T(8,128)(2,1)} %param.18) | copy-start | bytes 6291460
  100.3 6.2 %copy-start.6 = (bf16[256,2048]{1,0:T(8,128)(2,1)S(1)}, bf16[256,2048]{1,0:T(8,128)(2,1)}, u32[]{:S(2)}) copy-start(bf16[256,2048]{1,0:T(8,128)(2,1)} %param.19) | copy-start | bytes 3145732
  100.3 24.7 %collective-permute-start.22 = (bf16[4,1024,128]{2,1,0:T(8,128)(2,1)S(1)}, bf16[4,1024,128]{2,1,0:T(8,128)(2,1)}, u32[]{:S(2)}, u32[]{:S(2)}) collective-permute-start(bf16[4,1024,128]{2,1,0:T(8,128)(2,1)S(1)} %pad_maximum_fusion.2.refs_0_), channel_id=1, source_target_pairs={{0,2},{2,0},{4,6},{6,4},{8,10},{10,8},{12,14},{14,12},{16,18},{18,... | collective-permute-start | bytes 3145736 | tf_op jit(solution)/shard_map/ppermute | solution.py:75
  101.5 52.3 %collective-permute-start.17 = (bf16[4,128,1024]{2,1,0:T(8,128)(2,1)S(1)}, bf16[4,128,1024]{2,1,0:T(8,128)(2,1)}, u32[]{:S(2)}, u32[]{:S(2)}) collective-permute-start(bf16[4,128,1024]{2,1,0:T(8,128)(2,1)S(1)} %pad_maximum_fusion.1.refs_0_), channel_id=1, source_target_pairs={{0,4},{2,6},{4,0},{6,2},{8,12},{10,14},{12,8},{14,10},{16,20},{18,... | collective-permute-start | bytes 3145736 | tf_op jit(solution)/shard_map/ppermute | solution.py:75
  102.8 44.7 %collective-permute-start.24 = (bf16[4,1024,128]{2,1,0:T(8,128)(2,1)}, bf16[4,1024,128]{2,1,0:T(8,128)(2,1)}, u32[]{:S(2)}, u32[]{:S(2)}) collective-permute-start(bf16[4,1024,128]{2,1,0:T(8,128)(2,1)} %collective-permute-done.23.refs_2_), channel_id=1, source_target_pairs={{0,2},{2,0},{4,6},{6,4},{8,10},{10,8},{12,14},{14,12},{16,18},{18,... | collective-permute-start | bytes 3145736 | tf_op jit(solution)/shard_map/ppermute | solution.py:75
  103.9 49.9 %collective-permute-start.18 = (bf16[4,128,1024]{2,1,0:T(8,128)(2,1)}, bf16[4,128,1024]{2,1,0:T(8,128)(2,1)}, u32[]{:S(2)}, u32[]{:S(2)}) collective-permute-start(bf16[4,128,1024]{2,1,0:T(8,128)(2,1)} %collective-permute-done.16.refs_1_), channel_id=1, source_target_pairs={{0,4},{2,6},{4,0},{6,2},{8,12},{10,14},{12,8},{14,10},{16,20},{18,... | collective-permute-start | bytes 3145736 | tf_op jit(solution)/shard_map/ppermute | solution.py:75
  108.7 49.6 %collective-permute-start.31 = (bf16[256,1024]{1,0:T(8,128)(2,1)S(1)}, bf16[256,1024]{1,0:T(8,128)(2,1)}, u32[]{:S(2)}, u32[]{:S(2)}) collective-permute-start(bf16[256,1024]{1,0:T(8,128)(2,1)S(1)} %get-tuple-element.10), channel_id=1, source_target_pairs={{0,24},{2,26},{4,28},{6,30},{8,16},{10,18},{12,20},{14,22},{16,8},... | collective-permute-start | bytes 1572872 | tf_op jit(solution)/shard_map/ppermute | solution.py:75
  125.0 41.3 %collective-permute-start.27 = (bf16[256,1024]{1,0:T(8,128)(2,1)S(1)}, bf16[256,1024]{1,0:T(8,128)(2,1)}, u32[]{:S(2)}, u32[]{:S(2)}) collective-permute-start(bf16[256,1024]{1,0:T(8,128)(2,1)S(1)} %get-tuple-element.10), channel_id=1, source_target_pairs={{0,16},{2,18},{4,20},{6,22},{8,24},{10,26},{12,28},{14,30},{16,0},... | collective-permute-start | bytes 1572872 | tf_op jit(solution)/shard_map/ppermute | solution.py:75
  147.5 19.3 %collective-permute-start.11 = (bf16[256,1024]{1,0:T(8,128)(2,1)S(1)}, bf16[256,1024]{1,0:T(8,128)(2,1)}, u32[]{:S(2)}, u32[]{:S(2)}) collective-permute-start(bf16[256,1024]{1,0:T(8,128)(2,1)S(1)} %get-tuple-element.10), channel_id=1, source_target_pairs={{0,8},{2,10},{4,12},{6,14},{8,0},{10,2},{12,4},{14,6},{16,24},{18,... | collective-permute-start | bytes 1572872 | tf_op jit(solution)/shard_map/ppermute | solution.py:75
  158.2 8.8 %collective-permute-start.32 = (bf16[256,1024]{1,0:T(8,128)(2,1)}, bf16[256,1024]{1,0:T(8,128)(2,1)S(1)}, u32[]{:S(2)}, u32[]{:S(2)}) collective-permute-start(bf16[256,1024]{1,0:T(8,128)(2,1)} %collective-permute-done.31), channel_id=1, source_target_pairs={{0,1},{1,0},{2,3},{3,2},{4,5},{5,4},{6,7},{7,6},{8,9},{9,8},{10,11... | collective-permute-start | bytes 1572872 | tf_op jit(solution)/shard_map/ppermute | solution.py:75
  165.3 1.7 copy-start.7
  166.2 30.0 %collective-permute-start.35 = (bf16[256,1024]{1,0:T(8,128)(2,1)}, bf16[256,1024]{1,0:T(8,128)(2,1)}, u32[]{:S(2)}, u32[]{:S(2)}) collective-permute-start(bf16[256,1024]{1,0:T(8,128)(2,1)} %slice.121), channel_id=1, source_target_pairs={{0,1},{1,0},{2,3},{3,2},{4,5},{5,4},{6,7},{7,6},{8,9},{9,8},{10,11... | collective-permute-start | bytes 1572872 | tf_op jit(solution)/shard_map/ppermute | solution.py:75
  166.2 7.8 %collective-permute-start.28 = (bf16[256,1024]{1,0:T(8,128)(2,1)}, bf16[256,1024]{1,0:T(8,128)(2,1)}, u32[]{:S(2)}, u32[]{:S(2)}) collective-permute-start(bf16[256,1024]{1,0:T(8,128)(2,1)} %collective-permute-done.27), channel_id=1, source_target_pairs={{0,1},{1,0},{2,3},{3,2},{4,5},{5,4},{6,7},{7,6},{8,9},{9,8},{10,11... | collective-permute-start | bytes 1572872 | tf_op jit(solution)/shard_map/ppermute | solution.py:75
  166.8 14.6 %collective-permute-start.12 = (bf16[256,1024]{1,0:T(8,128)(2,1)}, bf16[256,1024]{1,0:T(8,128)(2,1)}, u32[]{:S(2)}, u32[]{:S(2)}) collective-permute-start(bf16[256,1024]{1,0:T(8,128)(2,1)} %collective-permute-done.11), channel_id=1, source_target_pairs={{0,1},{1,0},{2,3},{3,2},{4,5},{5,4},{6,7},{7,6},{8,9},{9,8},{10,11... | collective-permute-start | bytes 1572872 | tf_op jit(solution)/shard_map/ppermute | solution.py:75
  173.9 16.0 %collective-permute-start.33 = (bf16[256,1024]{1,0:T(8,128)(2,1)}, bf16[256,1024]{1,0:T(8,128)(2,1)S(1)}, u32[]{:S(2)}, u32[]{:S(2)}) collective-permute-start(bf16[256,1024]{1,0:T(8,128)(2,1)} %slice.119), channel_id=1, source_target_pairs={{0,1},{1,0},{2,3},{3,2},{4,5},{5,4},{6,7},{7,6},{8,9},{9,8},{10,11... | collective-permute-start | bytes 1572872 | tf_op jit(solution)/shard_map/ppermute | solution.py:75
  181.1 10.6 %collective-permute-start.29 = (bf16[256,1024]{1,0:T(8,128)(2,1)}, bf16[256,1024]{1,0:T(8,128)(2,1)}, u32[]{:S(2)}, u32[]{:S(2)}) collective-permute-start(bf16[256,1024]{1,0:T(8,128)(2,1)} %slice.117), channel_id=1, source_target_pairs={{0,1},{1,0},{2,3},{3,2},{4,5},{5,4},{6,7},{7,6},{8,9},{9,8},{10,11... | collective-permute-start | bytes 1572872 | tf_op jit(solution)/shard_map/ppermute | solution.py:75
  188.4 7.2 %copy-start.5 = (bf16[256,2048]{1,0:T(8,128)(2,1)S(1)}, bf16[256,2048]{1,0:T(8,128)(2,1)}, u32[]{:S(2)}) copy-start(bf16[256,2048]{1,0:T(8,128)(2,1)} %convolution_convert_fusion.5) | copy-start | bytes 3145732
  189.6 46.8 %copy-start.8 = (bf16[256,2048]{1,0:T(8,128)(2,1)S(1)}, bf16[256,2048]{1,0:T(8,128)(2,1)}, u32[]{:S(2)}) copy-start(bf16[256,2048]{1,0:T(8,128)(2,1)} %copy-done.7) | copy-start | bytes 3145732
  189.6 6.1 %collective-permute-start.25 = (bf16[256,1024]{1,0:T(8,128)(2,1)S(1)}, bf16[256,1024]{1,0:T(8,128)(2,1)S(1)}, u32[]{:S(2)}, u32[]{:S(2)}) collective-permute-start(bf16[256,1024]{1,0:T(8,128)(2,1)S(1)} %slice.115), channel_id=1, source_target_pairs={{0,1},{1,0},{2,3},{3,2},{4,5},{5,4},{6,7},{7,6},{8,9},{9,8},{10,11... | collective-permute-start | bytes 1572872 | tf_op jit(solution)/shard_map/ppermute | solution.py:75
  190.1 35.8 %collective-permute-start.34 = (bf16[256,1024]{1,0:T(8,128)(2,1)S(1)}, bf16[256,1024]{1,0:T(8,128)(2,1)S(1)}, u32[]{:S(2)}, u32[]{:S(2)}) collective-permute-start(bf16[256,1024]{1,0:T(8,128)(2,1)S(1)} %add_convert_fusion.2), channel_id=1, source_target_pairs={{0,24},{2,26},{4,28},{6,30},{8,16},{10,18},{12,20},{14,22},{16,8},... | collective-permute-start | bytes 1572872 | tf_op jit(solution)/shard_map/ppermute | solution.py:75
  192.9 43.5 %collective-permute-start.30 = (bf16[256,1024]{1,0:T(8,128)(2,1)S(1)}, bf16[256,1024]{1,0:T(8,128)(2,1)S(1)}, u32[]{:S(2)}, u32[]{:S(2)}) collective-permute-start(bf16[256,1024]{1,0:T(8,128)(2,1)S(1)} %add_convert_fusion.3), channel_id=1, source_target_pairs={{0,16},{2,18},{4,20},{6,22},{8,24},{10,26},{12,28},{14,30},{16,0},... | collective-permute-start | bytes 1572872 | tf_op jit(solution)/shard_map/ppermute | solution.py:75
  195.9 40.5 %collective-permute-start.26 = (bf16[256,1024]{1,0:T(8,128)(2,1)S(1)}, bf16[256,1024]{1,0:T(8,128)(2,1)S(1)}, u32[]{:S(2)}, u32[]{:S(2)}) collective-permute-start(bf16[256,1024]{1,0:T(8,128)(2,1)S(1)} %add_convert_fusion.4), channel_id=1, source_target_pairs={{0,8},{2,10},{4,12},{6,14},{8,0},{10,2},{12,4},{14,6},{16,24},{18,... | collective-permute-start | bytes 1572872 | tf_op jit(solution)/shard_map/ppermute | solution.py:75
  196.2 45.0 %dynamic-slice-start = ((f32[2048]{0:T(1024)}, s32[]{:T(128)}), f32[1024]{0:T(1024)S(1)}, s32[]{:S(2)}) async-start(f32[2048]{0:T(1024)} %param.25, s32[]{:T(128)} %select_n.249), calls=%async_computation | async-start | bytes 8704 | tf_op jit(solution)/shard_map/dynamic_slice | solution.py:70
  196.2 45.0 %dynamic-slice-start.1 = ((f32[2048]{0:T(1024)}, s32[]{:T(128)}), f32[1024]{0:T(1024)S(1)}, s32[]{:S(2)}) async-start(f32[2048]{0:T(1024)} %param.24, s32[]{:T(128)} %select_n.249), calls=%async_computation.1 | async-start | bytes 8704 | tf_op jit(solution)/shard_map/dynamic_slice | solution.py:70
  (4 other events, 3.8 us)

commit v3 on v2

--- a/solution.py
+++ b/solution.py
@@ -250,7 +250,7 @@
     normed_own = take_cols(full_rows, core * col_width, col_width)
 
     ffn_cols = jnp.zeros((tok_rows, col_width), jnp.float32)
-    for d in [*range(1, split), 0]:
+    for d in [*range(2, split), 1, 0][-split:]:
         if d == 0:
             pieces = [
                 take_cols(full_rows, (core ^ e) * col_width, col_width) for e in range(n_tp)
@@ -271,7 +271,8 @@
                 piece = swap(piece, "tp", e)
             cols = cols + piece.astype(jnp.float32)
         if d:
-            cols = swap(cols.astype(jnp.bfloat16), "sp", d * low_count).astype(jnp.float32)
+            cols = swap(cols.astype(jnp.bfloat16), "sp", d * low_count)
+            cols = cols.astype(jnp.float32)
         ffn_cols = ffn_cols + cols
 
     second = ALPHA * normed_own.astype(jnp.float32) + ffn_cols

time: 246 us -> 255 us (1.037)
  waiting for transfers between devices: 108 us -> 117 us
    ppermute x36, waiting for transfers between devices: 108 us -> 117 us  [swap(): lax.ppermute(array_in, axis_name, [(i, i ^ offset) for i in range(size)])]
  transfers between devices with their start and end apart: 36 -> 36, of which waited for: 13 -> 15; matrix products, arithmetic and copies ran while one was open for 18% -> 17% of each run, Pallas kernels for 10% -> 10%
where the time goes in v3:
time: 255 us; the launch traced here: 251 us
  waiting for transfers between devices  117 us (46%)
  starting transfers between devices  56.9 us (22%)
  matrix products  28.2 us (11%)
  Pallas kernels  24.8 us (10%)
  other arithmetic  10.8 us (4%)
  local copies, waits for them, and re-layouts  9.75 us (4%)
  blocking collectives  3.75 us (1%)
    ppermute x36, waiting for transfers between devices, swap(): lax.ppermute(array_in, axis_name, [(i, i ^ offset) for i in range(size)])  117 us
    ppermute x36, starting transfers between devices, swap(): lax.ppermute(array_in, axis_name, [(i, i ^ offset) for i in range(size)])  56.9 us
    dot_general x4, matrix products, local(): jnp.dot(hidden, down_own, preferred_element_type=jnp.float32)  24.9 us
    pallas_call x1, Pallas kernels, attend(): pl.pallas_call(attend_kernel, grid=(rows // block,), in_specs=[pl.BlockSp...  14.9 us
    pallas_call x2, Pallas kernels, place_blocks(): pl.pallas_call(kernel, in_specs=[pl.BlockSpec(memory_space=pltpu.SMEM)] +...  9.85 us
  transfers between devices with their start and end apart: 36, of which 15 were waited for; matrix products, arithmetic and copies ran while one was open for 17% of the time, Pallas kernels for 10%

profile of v3, /device:TPU:9, one launch (start us, length us, event | category | flops | bytes accessed | tf_op | source)
XLA Modules:
  0.0 251.3 jit_solution(5774628958312405749)
XLA Ops:
  3.3 1.4 collective-permute-start.2
  5.9 1.2 collective-permute-start
  7.2 1.2 collective-permute-start.10
  9.3 1.2 collective-permute-start.21
  10.8 2.9 %collective-permute-done.2 = bf16[1,256,256]{2,1,0:T(8,128)(2,1)} collective-permute-done((bf16[1,256,256]{2,1,0:T(8,128)(2,1)S(1)}, bf16[1,256,256]{2,1,0:T(8,128)(2,1)}, u32[]{:S(2)}, u32[]{:S(2)}) %collective-permute-start.2) | collective-permute-done | bytes 131104 | tf_op jit(solution)/shard_map/ppermute | solution.py:75
  13.6 1.9 collective-permute-done.1
  15.6 13.3 %collective-permute-start.19 = (bf16[1024,128]{1,0:T(8,128)(2,1)S(1)}, bf16[1024,128]{1,0:T(8,128)(2,1)S(1)}, u32[]{:S(2)}, u32[]{:S(2)}) collective-permute-start(bf16[1024,128]{1,0:T(8,128)(2,1)S(1)} %get-tuple-element.17), channel_id=1, source_target_pairs={{0,8},{2,10},{4,12},{6,14},{8,0},{10,2},{12,4},{14,6},{16,24},{18,... | collective-permute-start | bytes 786440 | tf_op jit(solution)/shard_map/ppermute | solution.py:75
  30.7 5.1 %collective-permute-done.21 = bf16[1024,128]{1,0:T(8,128)(2,1)} collective-permute-done((bf16[1024,128]{1,0:T(8,128)(2,1)}, bf16[1024,128]{1,0:T(8,128)(2,1)}, u32[]{:S(2)}, u32[]{:S(2)}) %collective-permute-start.21) | collective-permute-done | bytes 262176 | tf_op jit(solution)/shard_map/ppermute | solution.py:75
  35.8 1.2 collective-permute-start.3
  37.0 6.4 %collective-permute-done.20 = bf16[1024,128]{1,0:T(8,128)(2,1)S(1)} collective-permute-done((bf16[1024,128]{1,0:T(8,128)(2,1)}, bf16[1024,128]{1,0:T(8,128)(2,1)S(1)}, u32[]{:S(2)}, u32[]{:S(2)}) %collective-permute-start.20) | collective-permute-done | bytes 262176 | tf_op jit(solution)/shard_map/ppermute | solution.py:75
  43.4 3.0 %collective-permute-start.14 = (bf16[128,1024]{1,0:T(8,128)(2,1)S(1)}, bf16[128,1024]{1,0:T(8,128)(2,1)S(1)}, u32[]{:S(2)}, u32[]{:S(2)}) collective-permute-start(bf16[128,1024]{1,0:T(8,128)(2,1)S(1)} %get-tuple-element.15), channel_id=1, source_target_pairs={{0,16},{2,18},{4,20},{6,22},{8,24},{10,26},{12,28},{14,30},{16,0},... | collective-permute-start | bytes 786440 | tf_op jit(solution)/shard_map/ppermute | solution.py:75
  46.4 8.7 %collective-permute-done.15 = bf16[128,1024]{1,0:T(8,128)(2,1)S(1)} collective-permute-done((bf16[128,1024]{1,0:T(8,128)(2,1)S(1)}, bf16[128,1024]{1,0:T(8,128)(2,1)S(1)}, u32[]{:S(2)}, u32[]{:S(2)}) %collective-permute-start.15) | collective-permute-done | bytes 262176 | tf_op jit(solution)/shard_map/ppermute | solution.py:75
  55.2 1.2 collective-permute-start.4
  57.7 2.4 collective-permute-done.14
  60.2 1.2 collective-permute-start.23
  61.6 1.3 collective-permute-start.16
  62.9 3.0 %collective-permute-done.5 = bf16[1,1024,128]{2,1,0:T(8,128)(2,1)} collective-permute-done((bf16[1,1024,128]{2,1,0:T(8,128)(2,1)}, bf16[1,1024,128]{2,1,0:T(8,128)(2,1)}, u32[]{:S(2)}, u32[]{:S(2)}) %collective-permute-start.5) | collective-permute-done | bytes 262176 | tf_op jit(solution)/shard_map/ppermute | solution.py:75
  65.9 2.1 pad_maximum_fusion
  68.0 14.9 %shard_map.127 = bf16[1024,128]{1,0:T(8,128)(2,1)} custom-call(bf16[1024,128]{1,0:T(8,128)(2,1)} %get-tuple-element.26.q_ref, bf16[4096,128]{1,0:T(8,128)(2,1)} %bitcast.62), custom_call_target="tpu_custom_call" | custom-call | tf_op jit(solution)/shard_map/pallas_call | solution.py:146
  84.0 3.0 %collective-permute-start.7 = (bf16[256,128]{1,0:T(8,128)(2,1)S(1)}, bf16[256,128]{1,0:T(8,128)(2,1)S(1)}, u32[]{:S(2)}, u32[]{:S(2)}) collective-permute-start(bf16[256,128]{1,0:T(8,128)(2,1)S(1)} %get-tuple-element.34), channel_id=1, source_target_pairs={{0,16},{2,18},{4,20},{6,22},{8,24},{10,26},{12,28},{14,30},{16,0},... | collective-permute-start | bytes 196616 | tf_op jit(solution)/shard_map/ppermute | solution.py:75
  87.5 1.8 collective-permute-start.8
  89.4 2.3 collective-permute-done.8
  91.7 8.6 %collective-permute-start.9 = (bf16[256,512]{1,0:T(8,128)(2,1)S(1)}, bf16[256,512]{1,0:T(8,128)(2,1)S(1)}, u32[]{:S(2)}, u32[]{:S(2)}) collective-permute-start(bf16[256,512]{1,0:T(8,128)(2,1)S(1)} %constant_dynamic-update-slice_fusion.1), channel_id=1, source_target_pairs={{0,1},{1,0},{2,3},{3,2},{4,5},{5,4},{6,7},{7,6},{8,9},{9,8},{10,11... | collective-permute-start | bytes 786440 | tf_op jit(solution)/shard_map/ppermute | solution.py:75
  100.3 1.2 collective-permute-start.22
  101.5 1.3 collective-permute-start.17
  102.8 1.2 collective-permute-start.24
  104.1 2.3 fusion.3
  110.4 14.6 %collective-permute-done.22.refs_1_ = bf16[4,1024,128]{2,1,0:T(8,128)(2,1)} collective-permute-done((bf16[4,1024,128]{2,1,0:T(8,128)(2,1)S(1)}, bf16[4,1024,128]{2,1,0:T(8,128)(2,1)}, u32[]{:S(2)}, u32[]{:S(2)}) %collective-permute-start.22) | collective-permute-done | bytes 1048608 | tf_op jit(solution)/shard_map/ppermute | solution.py:75
  125.0 1.5 collective-permute-start.27
  126.5 21.0 %collective-permute-done.24.refs_3_ = bf16[4,1024,128]{2,1,0:T(8,128)(2,1)} collective-permute-done((bf16[4,1024,128]{2,1,0:T(8,128)(2,1)}, bf16[4,1024,128]{2,1,0:T(8,128)(2,1)}, u32[]{:S(2)}, u32[]{:S(2)}) %collective-permute-start.24) | collective-permute-done | bytes 1048608 | tf_op jit(solution)/shard_map/ppermute | solution.py:75
  147.5 2.1 collective-permute-start.11
  149.6 5.4 %shard_map.129 = bf16[1024,2048]{1,0:T(8,128)(2,1)} custom-call(s32[16]{0:T(128)} %stack.134.starts_ref, bf16[4,1024,128]{2,1,0:T(8,128)(2,1)} %copy-done, bf16[4,1024,128]{2,1,0:T(8,128)(2,1)} %collective-permute-done.22.refs_1_, bf16[4,1024,128]{2,1,0:T(8,128)(2,1)} %collective-permute-done.23.refs_2_, bf16[4,1024,128]{2,1,0:T(8,128)(2,1)} %collective-permute-done.24.refs_3_), custom_call_target="tpu_custom_call" | custom-call | tf_op jit(solution)/shard_map/pallas_call | solution.py:116
  155.0 4.5 %shard_map.128 = bf16[2048,1024]{1,0:T(8,128)(2,1)} custom-call(s32[16]{0:T(128)} %stack.134.starts_ref, bf16[4,128,1024]{2,1,0:T(8,128)(2,1)} %copy-done.1, bf16[4,128,1024]{2,1,0:T(8,128)(2,1)} %collective-permute-done.16.refs_1_, bf16[4,128,1024]{2,1,0:T(8,128)(2,1)} %collective-permute-done.17.refs_2_, bf16[4,128,1024]{2,1,0:T(8,128)(2,1)} %collective-permute-done.18.refs_3_), custom_call_target="tpu_custom_call" | custom-call | tf_op jit(solution)/shard_map/pallas_call | solution.py:116
  159.4 1.3 collective-permute-start.32
  160.7 5.8 %convolution_convert_fusion.2 = bf16[256,2048]{1,0:T(8,128)(2,1)S(1)} fusion(bf16[1024,2048]{1,0:T(8,128)(2,1)} %shard_map.129, bf16[2048,1024]{1,0:T(8,128)(2,1)} %shard_map.128, bf16[256,1024]{1,0:T(8,128)(2,1)S(1)} %get-tuple-element.11, bf16[256,1024]{1,0:T(8,128)(2,1)S(1)} %get-tuple-element.10), kind=kOutput, calls=%fused_computation.2 | convolution fusion | flops 2150891520 | bytes 10485760 | tf_op jit(solution)/shard_map/dot_general | solution.py:264
  168.0 4.2 %collective-permute-done.11 = bf16[256,1024]{1,0:T(8,128)(2,1)} collective-permute-done((bf16[256,1024]{1,0:T(8,128)(2,1)S(1)}, bf16[256,1024]{1,0:T(8,128)(2,1)}, u32[]{:S(2)}, u32[]{:S(2)}) %collective-permute-start.11) | collective-permute-done | bytes 524320 | tf_op jit(solution)/shard_map/ppermute | solution.py:75
  173.0 6.0 %convolution_convert_fusion.3 = bf16[256,2048]{1,0:T(8,128)(2,1)S(1)} fusion(bf16[1024,2048]{1,0:T(8,128)(2,1)} %shard_map.129, bf16[2048,1024]{1,0:T(8,128)(2,1)} %shard_map.128, bf16[256,1024]{1,0:T(8,128)(2,1)S(1)} %collective-permute-done.32, bf16[256,1024]{1,0:T(8,128)(2,1)} %collective-permute-done.31), kind=kOutput, calls=%fused_computation.3 | convolution fusion | flops 2150891520 | bytes 10485760 | tf_op jit(solution)/shard_map/dot_general | solution.py:264
  179.8 6.1 %convolution_convert_fusion.4 = bf16[256,2048]{1,0:T(8,128)(2,1)S(1)} fusion(bf16[1024,2048]{1,0:T(8,128)(2,1)} %shard_map.129, bf16[2048,1024]{1,0:T(8,128)(2,1)} %shard_map.128, bf16[256,1024]{1,0:T(8,128)(2,1)} %collective-permute-done.28, bf16[256,1024]{1,0:T(8,128)(2,1)} %collective-permute-done.27), kind=kOutput, calls=%fused_computation.4 | convolution fusion | flops 2150891520 | bytes 10485760 | tf_op jit(solution)/shard_map/dot_general | solution.py:264
  187.3 7.1 %convolution_convert_fusion.5 = bf16[256,2048]{1,0:T(8,128)(2,1)} fusion(bf16[1024,2048]{1,0:T(8,128)(2,1)} %shard_map.129, bf16[2048,1024]{1,0:T(8,128)(2,1)} %shard_map.128, bf16[256,1024]{1,0:T(8,128)(2,1)} %collective-permute-done.12, bf16[256,1024]{1,0:T(8,128)(2,1)} %collective-permute-done.11), kind=kOutput, calls=%fused_computation.5 | convolution fusion | flops 2150891520 | bytes 10485760 | tf_op jit(solution)/shard_map/dot_general | solution.py:264
  194.3 1.2 slice.115
  195.8 2.1 collective-permute-start.34
  197.9 1.2 add_convert_fusion.3
  199.1 1.5 collective-permute-start.30
  201.6 8.1 %collective-permute-done.34 = bf16[256,1024]{1,0:T(8,128)(2,1)S(1)} collective-permute-done((bf16[256,1024]{1,0:T(8,128)(2,1)S(1)}, bf16[256,1024]{1,0:T(8,128)(2,1)S(1)}, u32[]{:S(2)}, u32[]{:S(2)}) %collective-permute-start.34) | collective-permute-done | bytes 524320 | tf_op jit(solution)/shard_map/ppermute | solution.py:75
  209.7 24.7 %collective-permute-done.30 = bf16[256,1024]{1,0:T(8,128)(2,1)S(1)} collective-permute-done((bf16[256,1024]{1,0:T(8,128)(2,1)S(1)}, bf16[256,1024]{1,0:T(8,128)(2,1)S(1)}, u32[]{:S(2)}, u32[]{:S(2)}) %collective-permute-start.30) | collective-permute-done | bytes 524320 | tf_op jit(solution)/shard_map/ppermute | solution.py:75
  234.4 10.5 %collective-permute-done.26 = bf16[256,1024]{1,0:T(8,128)(2,1)S(1)} collective-permute-done((bf16[256,1024]{1,0:T(8,128)(2,1)S(1)}, bf16[256,1024]{1,0:T(8,128)(2,1)S(1)}, u32[]{:S(2)}, u32[]{:S(2)}) %collective-permute-start.26) | collective-permute-done | bytes 524320 | tf_op jit(solution)/shard_map/ppermute | solution.py:75
  244.9 1.6 fusion.60
  246.5 3.8 %all-reduce = (f32[256]{0:T(256)S(1)}, f32[256]{0:T(256)S(1)}) all-reduce(f32[256]{0:T(256)S(1)} %get-tuple-element.6, f32[256]{0:T(256)S(1)} %get-tuple-element.5), channel_id=1, replica_groups=mesh['sp'=16,'tp'=2] {'tp'}, use_global_device_ids=true, to_apply=%region_7.8 | all-reduce | flops 512 | bytes 4096 | tf_op jit(solution)/shard_map/psum | solution.py:279
  (119 shorter events, 21.1 us)
Async XLA Ops:
  0.0 2.4 copy-start.9
  2.4 6.0 %copy-start.3 = (bf16[4096,128]{1,0:T(8,128)(2,1)S(1)}, bf16[4096,128]{1,0:T(8,128)(2,1)}, u32[]{:S(2)}) copy-start(bf16[4096,128]{1,0:T(8,128)(2,1)} %param.23) | copy-start | bytes 3145732
  3.1 7.5 %copy-start.4 = (bf16[128,4096]{1,0:T(8,128)(2,1)S(1)}, bf16[128,4096]{1,0:T(8,128)(2,1)}, u32[]{:S(2)}) copy-start(bf16[128,4096]{1,0:T(8,128)(2,1)} %param.22) | copy-start | bytes 3145732
  3.3 10.4 %collective-permute-start.2 = (bf16[1,256,256]{2,1,0:T(8,128)(2,1)S(1)}, bf16[1,256,256]{2,1,0:T(8,128)(2,1)}, u32[]{:S(2)}, u32[]{:S(2)}) collective-permute-start(bf16[1,256,256]{2,1,0:T(8,128)(2,1)S(1)} %bitcast.74), channel_id=1, source_target_pairs={{0,24},{2,26},{4,28},{6,30},{8,16},{10,18},{12,20},{14,22},{16,8},... | collective-permute-start | bytes 393224 | tf_op jit(solution)/shard_map/ppermute | solution.py:75
  4.7 10.8 %collective-permute-start.1 = (bf16[1,256,256]{2,1,0:T(8,128)(2,1)S(1)}, bf16[1,256,256]{2,1,0:T(8,128)(2,1)}, u32[]{:S(2)}, u32[]{:S(2)}) collective-permute-start(bf16[1,256,256]{2,1,0:T(8,128)(2,1)S(1)} %bitcast.73), channel_id=1, source_target_pairs={{0,16},{2,18},{4,20},{6,22},{8,24},{10,26},{12,28},{14,30},{16,0},... | collective-permute-start | bytes 393224 | tf_op jit(solution)/shard_map/ppermute | solution.py:75
  5.9 22.9 %collective-permute-start = (bf16[1,256,256]{2,1,0:T(8,128)(2,1)S(1)}, bf16[1,256,256]{2,1,0:T(8,128)(2,1)S(1)}, u32[]{:S(2)}, u32[]{:S(2)}) collective-permute-start(bf16[1,256,256]{2,1,0:T(8,128)(2,1)S(1)} %bitcast.72), channel_id=1, source_target_pairs={{0,8},{2,10},{4,12},{6,14},{8,0},{10,2},{12,4},{14,6},{16,24},{18,... | collective-permute-start | bytes 393224 | tf_op jit(solution)/shard_map/ppermute | solution.py:75
  7.2 96.9 %collective-permute-start.10 = (bf16[512,2048]{1,0:T(8,128)(2,1)}, bf16[512,2048]{1,0:T(8,128)(2,1)}, u32[]{:S(2)}, u32[]{:S(2)}) collective-permute-start(bf16[512,2048]{1,0:T(8,128)(2,1)} %param.18), channel_id=1, source_target_pairs={{0,1},{1,0},{2,3},{3,2},{4,5},{5,4},{6,7},{7,6},{8,9},{9,8},{10,11... | collective-permute-start | bytes 6291464 | tf_op jit(solution)/shard_map/ppermute | solution.py:75
  9.3 26.5 %collective-permute-start.21 = (bf16[1024,128]{1,0:T(8,128)(2,1)}, bf16[1024,128]{1,0:T(8,128)(2,1)}, u32[]{:S(2)}, u32[]{:S(2)}) collective-permute-start(bf16[1024,128]{1,0:T(8,128)(2,1)} %get-tuple-element.18), channel_id=1, source_target_pairs={{0,24},{2,26},{4,28},{6,30},{8,16},{10,18},{12,20},{14,22},{16,8},... | collective-permute-start | bytes 786440 | tf_op jit(solution)/shard_map/ppermute | solution.py:75
  13.6 29.8 %collective-permute-start.20 = (bf16[1024,128]{1,0:T(8,128)(2,1)}, bf16[1024,128]{1,0:T(8,128)(2,1)S(1)}, u32[]{:S(2)}, u32[]{:S(2)}) collective-permute-start(bf16[1024,128]{1,0:T(8,128)(2,1)} %get-tuple-element.19), channel_id=1, source_target_pairs={{0,16},{2,18},{4,20},{6,22},{8,24},{10,26},{12,28},{14,30},{16,0},... | collective-permute-start | bytes 786440 | tf_op jit(solution)/shard_map/ppermute | solution.py:75
  15.6 30.9 %collective-permute-start.19 = (bf16[1024,128]{1,0:T(8,128)(2,1)S(1)}, bf16[1024,128]{1,0:T(8,128)(2,1)S(1)}, u32[]{:S(2)}, u32[]{:S(2)}) collective-permute-start(bf16[1024,128]{1,0:T(8,128)(2,1)S(1)} %get-tuple-element.17), channel_id=1, source_target_pairs={{0,8},{2,10},{4,12},{6,14},{8,0},{10,2},{12,4},{14,6},{16,24},{18,... | collective-permute-start | bytes 786440 | tf_op jit(solution)/shard_map/ppermute | solution.py:75
  28.9 26.3 %collective-permute-start.15 = (bf16[128,1024]{1,0:T(8,128)(2,1)S(1)}, bf16[128,1024]{1,0:T(8,128)(2,1)S(1)}, u32[]{:S(2)}, u32[]{:S(2)}) collective-permute-start(bf16[128,1024]{1,0:T(8,128)(2,1)S(1)} %get-tuple-element.14), channel_id=1, source_target_pairs={{0,24},{2,26},{4,28},{6,30},{8,16},{10,18},{12,20},{14,22},{16,8},... | collective-permute-start | bytes 786440 | tf_op jit(solution)/shard_map/ppermute | solution.py:75
  35.8 20.6 %collective-permute-start.3 = (bf16[1,1024,128]{2,1,0:T(8,128)(2,1)S(1)}, bf16[1,1024,128]{2,1,0:T(8,128)(2,1)}, u32[]{:S(2)}, u32[]{:S(2)}) collective-permute-start(bf16[1,1024,128]{2,1,0:T(8,128)(2,1)S(1)} %get-tuple-element.25), channel_id=1, source_target_pairs={{0,2},{2,0},{4,6},{6,4},{8,10},{10,8},{12,14},{14,12},{16,18},{18,... | collective-permute-start | bytes 786440 | tf_op jit(solution)/shard_map/ppermute | solution.py:75
  43.4 16.7 %collective-permute-start.14 = (bf16[128,1024]{1,0:T(8,128)(2,1)S(1)}, bf16[128,1024]{1,0:T(8,128)(2,1)S(1)}, u32[]{:S(2)}, u32[]{:S(2)}) collective-permute-start(bf16[128,1024]{1,0:T(8,128)(2,1)S(1)} %get-tuple-element.15), channel_id=1, source_target_pairs={{0,16},{2,18},{4,20},{6,22},{8,24},{10,26},{12,28},{14,30},{16,0},... | collective-permute-start | bytes 786440 | tf_op jit(solution)/shard_map/ppermute | solution.py:75
  46.4 15.0 %collective-permute-start.13 = (bf16[128,1024]{1,0:T(8,128)(2,1)S(1)}, bf16[128,1024]{1,0:T(8,128)(2,1)S(1)}, u32[]{:S(2)}, u32[]{:S(2)}) collective-permute-start(bf16[128,1024]{1,0:T(8,128)(2,1)S(1)} %get-tuple-element.13), channel_id=1, source_target_pairs={{0,8},{2,10},{4,12},{6,14},{8,0},{10,2},{12,4},{14,6},{16,24},{18,... | collective-permute-start | bytes 786440 | tf_op jit(solution)/shard_map/ppermute | solution.py:75
  55.2 7.7 %collective-permute-start.4 = (bf16[1,1024,128]{2,1,0:T(8,128)(2,1)S(1)}, bf16[1,1024,128]{2,1,0:T(8,128)(2,1)S(1)}, u32[]{:S(2)}, u32[]{:S(2)}) collective-permute-start(bf16[1,1024,128]{2,1,0:T(8,128)(2,1)S(1)} %get-tuple-element.25), channel_id=1, source_target_pairs={{0,4},{2,6},{4,0},{6,2},{8,12},{10,14},{12,8},{14,10},{16,20},{18,... | collective-permute-start | bytes 786440 | tf_op jit(solution)/shard_map/ppermute | solution.py:75
  56.4 9.5 %collective-permute-start.5 = (bf16[1,1024,128]{2,1,0:T(8,128)(2,1)}, bf16[1,1024,128]{2,1,0:T(8,128)(2,1)}, u32[]{:S(2)}, u32[]{:S(2)}) collective-permute-start(bf16[1,1024,128]{2,1,0:T(8,128)(2,1)} %collective-permute-done.3), channel_id=1, source_target_pairs={{0,4},{2,6},{4,0},{6,2},{8,12},{10,14},{12,8},{14,10},{16,20},{18,... | collective-permute-start | bytes 786440 | tf_op jit(solution)/shard_map/ppermute | solution.py:75
  57.7 42.5 %copy-start = (bf16[4,1024,128]{2,1,0:T(8,128)(2,1)}, bf16[4,1024,128]{2,1,0:T(8,128)(2,1)S(1)}, u32[]{:S(2)}) copy-start(bf16[4,1024,128]{2,1,0:T(8,128)(2,1)S(1)} %pad_maximum_fusion.2.refs_0_) | copy-start | bytes 3145732
  60.2 42.6 %collective-permute-start.23 = (bf16[4,1024,128]{2,1,0:T(8,128)(2,1)S(1)}, bf16[4,1024,128]{2,1,0:T(8,128)(2,1)}, u32[]{:S(2)}, u32[]{:S(2)}) collective-permute-start(bf16[4,1024,128]{2,1,0:T(8,128)(2,1)S(1)} %pad_maximum_fusion.2.refs_0_), channel_id=1, source_target_pairs={{0,4},{2,6},{4,0},{6,2},{8,12},{10,14},{12,8},{14,10},{16,20},{18,... | collective-permute-start | bytes 3145736 | tf_op jit(solution)/shard_map/ppermute | solution.py:75
  61.6 39.9 %copy-start.1 = (bf16[4,128,1024]{2,1,0:T(8,128)(2,1)}, bf16[4,128,1024]{2,1,0:T(8,128)(2,1)S(1)}, u32[]{:S(2)}) copy-start(bf16[4,128,1024]{2,1,0:T(8,128)(2,1)S(1)} %pad_maximum_fusion.1.refs_0_) | copy-start | bytes 3145732
  61.6 42.3 %collective-permute-start.16 = (bf16[4,128,1024]{2,1,0:T(8,128)(2,1)S(1)}, bf16[4,128,1024]{2,1,0:T(8,128)(2,1)}, u32[]{:S(2)}, u32[]{:S(2)}) collective-permute-start(bf16[4,128,1024]{2,1,0:T(8,128)(2,1)S(1)} %pad_maximum_fusion.1.refs_0_), channel_id=1, source_target_pairs={{0,2},{2,0},{4,6},{6,4},{8,10},{10,8},{12,14},{14,12},{16,18},{18,... | collective-permute-start | bytes 3145736 | tf_op jit(solution)/shard_map/ppermute | solution.py:75
  83.9 3.6 %collective-permute-start.6 = (bf16[256,128]{1,0:T(8,128)(2,1)S(1)}, bf16[256,128]{1,0:T(8,128)(2,1)S(1)}, u32[]{:S(2)}, u32[]{:S(2)}) collective-permute-start(bf16[256,128]{1,0:T(8,128)(2,1)S(1)} %get-tuple-element.35), channel_id=1, source_target_pairs={{0,8},{2,10},{4,12},{6,14},{8,0},{10,2},{12,4},{14,6},{16,24},{18,... | collective-permute-start | bytes 196616 | tf_op jit(solution)/shard_map/ppermute | solution.py:75
  84.0 5.3 %collective-permute-start.7 = (bf16[256,128]{1,0:T(8,128)(2,1)S(1)}, bf16[256,128]{1,0:T(8,128)(2,1)S(1)}, u32[]{:S(2)}, u32[]{:S(2)}) collective-permute-start(bf16[256,128]{1,0:T(8,128)(2,1)S(1)} %get-tuple-element.34), channel_id=1, source_target_pairs={{0,16},{2,18},{4,20},{6,22},{8,24},{10,26},{12,28},{14,30},{16,0},... | collective-permute-start | bytes 196616 | tf_op jit(solution)/shard_map/ppermute | solution.py:75
  87.5 4.2 %collective-permute-start.8 = (bf16[256,128]{1,0:T(8,128)(2,1)S(1)}, bf16[256,128]{1,0:T(8,128)(2,1)S(1)}, u32[]{:S(2)}, u32[]{:S(2)}) collective-permute-start(bf16[256,128]{1,0:T(8,128)(2,1)S(1)} %get-tuple-element.33), channel_id=1, source_target_pairs={{0,24},{2,26},{4,28},{6,30},{8,16},{10,18},{12,20},{14,22},{16,8},... | collective-permute-start | bytes 196616 | tf_op jit(solution)/shard_map/ppermute | solution.py:75
  91.7 9.8 %collective-permute-start.9 = (bf16[256,512]{1,0:T(8,128)(2,1)S(1)}, bf16[256,512]{1,0:T(8,128)(2,1)S(1)}, u32[]{:S(2)}, u32[]{:S(2)}) collective-permute-start(bf16[256,512]{1,0:T(8,128)(2,1)S(1)} %constant_dynamic-update-slice_fusion.1), channel_id=1, source_target_pairs={{0,1},{1,0},{2,3},{3,2},{4,5},{5,4},{6,7},{7,6},{8,9},{9,8},{10,11... | collective-permute-start | bytes 786440 | tf_op jit(solution)/shard_map/ppermute | solution.py:75
  100.3 6.1 %copy-start.2 = (bf16[512,2048]{1,0:T(8,128)(2,1)S(1)}, bf16[512,2048]{1,0:T(8,128)(2,1)}, u32[]{:S(2)}) copy-start(bf16[512,2048]{1,0:T(8,128)(2,1)} %param.18) | copy-start | bytes 6291460
  100.3 6.2 %copy-start.6 = (bf16[256,2048]{1,0:T(8,128)(2,1)S(1)}, bf16[256,2048]{1,0:T(8,128)(2,1)}, u32[]{:S(2)}) copy-start(bf16[256,2048]{1,0:T(8,128)(2,1)} %param.19) | copy-start | bytes 3145732
  100.3 24.7 %collective-permute-start.22 = (bf16[4,1024,128]{2,1,0:T(8,128)(2,1)S(1)}, bf16[4,1024,128]{2,1,0:T(8,128)(2,1)}, u32[]{:S(2)}, u32[]{:S(2)}) collective-permute-start(bf16[4,1024,128]{2,1,0:T(8,128)(2,1)S(1)} %pad_maximum_fusion.2.refs_0_), channel_id=1, source_target_pairs={{0,2},{2,0},{4,6},{6,4},{8,10},{10,8},{12,14},{14,12},{16,18},{18,... | collective-permute-start | bytes 3145736 | tf_op jit(solution)/shard_map/ppermute | solution.py:75
  101.5 53.5 %collective-permute-start.17 = (bf16[4,128,1024]{2,1,0:T(8,128)(2,1)S(1)}, bf16[4,128,1024]{2,1,0:T(8,128)(2,1)}, u32[]{:S(2)}, u32[]{:S(2)}) collective-permute-start(bf16[4,128,1024]{2,1,0:T(8,128)(2,1)S(1)} %pad_maximum_fusion.1.refs_0_), channel_id=1, source_target_pairs={{0,4},{2,6},{4,0},{6,2},{8,12},{10,14},{12,8},{14,10},{16,20},{18,... | collective-permute-start | bytes 3145736 | tf_op jit(solution)/shard_map/ppermute | solution.py:75
  102.8 44.7 %collective-permute-start.24 = (bf16[4,1024,128]{2,1,0:T(8,128)(2,1)}, bf16[4,1024,128]{2,1,0:T(8,128)(2,1)}, u32[]{:S(2)}, u32[]{:S(2)}) collective-permute-start(bf16[4,1024,128]{2,1,0:T(8,128)(2,1)} %collective-permute-done.23.refs_2_), channel_id=1, source_target_pairs={{0,2},{2,0},{4,6},{6,4},{8,10},{10,8},{12,14},{14,12},{16,18},{18,... | collective-permute-start | bytes 3145736 | tf_op jit(solution)/shard_map/ppermute | solution.py:75
  103.9 51.1 %collective-permute-start.18 = (bf16[4,128,1024]{2,1,0:T(8,128)(2,1)}, bf16[4,128,1024]{2,1,0:T(8,128)(2,1)}, u32[]{:S(2)}, u32[]{:S(2)}) collective-permute-start(bf16[4,128,1024]{2,1,0:T(8,128)(2,1)} %collective-permute-done.16.refs_1_), channel_id=1, source_target_pairs={{0,4},{2,6},{4,0},{6,2},{8,12},{10,14},{12,8},{14,10},{16,20},{18,... | collective-permute-start | bytes 3145736 | tf_op jit(solution)/shard_map/ppermute | solution.py:75
  108.7 50.8 %collective-permute-start.31 = (bf16[256,1024]{1,0:T(8,128)(2,1)S(1)}, bf16[256,1024]{1,0:T(8,128)(2,1)}, u32[]{:S(2)}, u32[]{:S(2)}) collective-permute-start(bf16[256,1024]{1,0:T(8,128)(2,1)S(1)} %get-tuple-element.10), channel_id=1, source_target_pairs={{0,8},{2,10},{4,12},{6,14},{8,0},{10,2},{12,4},{14,6},{16,24},{18,... | collective-permute-start | bytes 1572872 | tf_op jit(solution)/shard_map/ppermute | solution.py:75
  125.0 42.5 %collective-permute-start.27 = (bf16[256,1024]{1,0:T(8,128)(2,1)S(1)}, bf16[256,1024]{1,0:T(8,128)(2,1)}, u32[]{:S(2)}, u32[]{:S(2)}) collective-permute-start(bf16[256,1024]{1,0:T(8,128)(2,1)S(1)} %get-tuple-element.10), channel_id=1, source_target_pairs={{0,24},{2,26},{4,28},{6,30},{8,16},{10,18},{12,20},{14,22},{16,8},... | collective-permute-start | bytes 1572872 | tf_op jit(solution)/shard_map/ppermute | solution.py:75
  147.5 24.7 %collective-permute-start.11 = (bf16[256,1024]{1,0:T(8,128)(2,1)S(1)}, bf16[256,1024]{1,0:T(8,128)(2,1)}, u32[]{:S(2)}, u32[]{:S(2)}) collective-permute-start(bf16[256,1024]{1,0:T(8,128)(2,1)S(1)} %get-tuple-element.10), channel_id=1, source_target_pairs={{0,16},{2,18},{4,20},{6,22},{8,24},{10,26},{12,28},{14,30},{16,0},... | collective-permute-start | bytes 1572872 | tf_op jit(solution)/shard_map/ppermute | solution.py:75
  159.4 13.5 %collective-permute-start.32 = (bf16[256,1024]{1,0:T(8,128)(2,1)}, bf16[256,1024]{1,0:T(8,128)(2,1)S(1)}, u32[]{:S(2)}, u32[]{:S(2)}) collective-permute-start(bf16[256,1024]{1,0:T(8,128)(2,1)} %collective-permute-done.31), channel_id=1, source_target_pairs={{0,1},{1,0},{2,3},{3,2},{4,5},{5,4},{6,7},{7,6},{8,9},{9,8},{10,11... | collective-permute-start | bytes 1572872 | tf_op jit(solution)/shard_map/ppermute | solution.py:75
  166.5 6.5 %copy-start.7 = (bf16[256,2048]{1,0:T(8,128)(2,1)}, bf16[256,2048]{1,0:T(8,128)(2,1)S(1)}, u32[]{:S(2)}) copy-start(bf16[256,2048]{1,0:T(8,128)(2,1)S(1)} %convolution_convert_fusion.2) | copy-start | bytes 3145732
  167.4 34.1 %collective-permute-start.35 = (bf16[256,1024]{1,0:T(8,128)(2,1)}, bf16[256,1024]{1,0:T(8,128)(2,1)}, u32[]{:S(2)}, u32[]{:S(2)}) collective-permute-start(bf16[256,1024]{1,0:T(8,128)(2,1)} %slice.121), channel_id=1, source_target_pairs={{0,1},{1,0},{2,3},{3,2},{4,5},{5,4},{6,7},{7,6},{8,9},{9,8},{10,11... | collective-permute-start | bytes 1572872 | tf_op jit(solution)/shard_map/ppermute | solution.py:75
  167.4 12.3 %collective-permute-start.28 = (bf16[256,1024]{1,0:T(8,128)(2,1)}, bf16[256,1024]{1,0:T(8,128)(2,1)}, u32[]{:S(2)}, u32[]{:S(2)}) collective-permute-start(bf16[256,1024]{1,0:T(8,128)(2,1)} %collective-permute-done.27), channel_id=1, source_target_pairs={{0,1},{1,0},{2,3},{3,2},{4,5},{5,4},{6,7},{7,6},{8,9},{9,8},{10,11... | collective-permute-start | bytes 1572872 | tf_op jit(solution)/shard_map/ppermute | solution.py:75
  172.2 15.1 %collective-permute-start.12 = (bf16[256,1024]{1,0:T(8,128)(2,1)}, bf16[256,1024]{1,0:T(8,128)(2,1)}, u32[]{:S(2)}, u32[]{:S(2)}) collective-permute-start(bf16[256,1024]{1,0:T(8,128)(2,1)} %collective-permute-done.11), channel_id=1, source_target_pairs={{0,1},{1,0},{2,3},{3,2},{4,5},{5,4},{6,7},{7,6},{8,9},{9,8},{10,11... | collective-permute-start | bytes 1572872 | tf_op jit(solution)/shard_map/ppermute | solution.py:75
  179.8 15.8 %collective-permute-start.33 = (bf16[256,1024]{1,0:T(8,128)(2,1)}, bf16[256,1024]{1,0:T(8,128)(2,1)S(1)}, u32[]{:S(2)}, u32[]{:S(2)}) collective-permute-start(bf16[256,1024]{1,0:T(8,128)(2,1)} %slice.119), channel_id=1, source_target_pairs={{0,1},{1,0},{2,3},{3,2},{4,5},{5,4},{6,7},{7,6},{8,9},{9,8},{10,11... | collective-permute-start | bytes 1572872 | tf_op jit(solution)/shard_map/ppermute | solution.py:75
  186.8 11.1 %collective-permute-start.29 = (bf16[256,1024]{1,0:T(8,128)(2,1)}, bf16[256,1024]{1,0:T(8,128)(2,1)}, u32[]{:S(2)}, u32[]{:S(2)}) collective-permute-start(bf16[256,1024]{1,0:T(8,128)(2,1)} %slice.117), channel_id=1, source_target_pairs={{0,1},{1,0},{2,3},{3,2},{4,5},{5,4},{6,7},{7,6},{8,9},{9,8},{10,11... | collective-permute-start | bytes 1572872 | tf_op jit(solution)/shard_map/ppermute | solution.py:75
  194.3 6.3 %copy-start.5 = (bf16[256,2048]{1,0:T(8,128)(2,1)S(1)}, bf16[256,2048]{1,0:T(8,128)(2,1)}, u32[]{:S(2)}) copy-start(bf16[256,2048]{1,0:T(8,128)(2,1)} %convolution_convert_fusion.5) | copy-start | bytes 3145732
  195.5 49.4 %copy-start.8 = (bf16[256,2048]{1,0:T(8,128)(2,1)S(1)}, bf16[256,2048]{1,0:T(8,128)(2,1)}, u32[]{:S(2)}) copy-start(bf16[256,2048]{1,0:T(8,128)(2,1)} %copy-done.7) | copy-start | bytes 3145732
  195.5 5.2 %collective-permute-start.25 = (bf16[256,1024]{1,0:T(8,128)(2,1)S(1)}, bf16[256,1024]{1,0:T(8,128)(2,1)S(1)}, u32[]{:S(2)}, u32[]{:S(2)}) collective-permute-start(bf16[256,1024]{1,0:T(8,128)(2,1)S(1)} %slice.115), channel_id=1, source_target_pairs={{0,1},{1,0},{2,3},{3,2},{4,5},{5,4},{6,7},{7,6},{8,9},{9,8},{10,11... | collective-permute-start | bytes 1572872 | tf_op jit(solution)/shard_map/ppermute | solution.py:75
  195.8 13.9 %collective-permute-start.34 = (bf16[256,1024]{1,0:T(8,128)(2,1)S(1)}, bf16[256,1024]{1,0:T(8,128)(2,1)S(1)}, u32[]{:S(2)}, u32[]{:S(2)}) collective-permute-start(bf16[256,1024]{1,0:T(8,128)(2,1)S(1)} %add_convert_fusion.2), channel_id=1, source_target_pairs={{0,8},{2,10},{4,12},{6,14},{8,0},{10,2},{12,4},{14,6},{16,24},{18,... | collective-permute-start | bytes 1572872 | tf_op jit(solution)/shard_map/ppermute | solution.py:75
  199.1 35.3 %collective-permute-start.30 = (bf16[256,1024]{1,0:T(8,128)(2,1)S(1)}, bf16[256,1024]{1,0:T(8,128)(2,1)S(1)}, u32[]{:S(2)}, u32[]{:S(2)}) collective-permute-start(bf16[256,1024]{1,0:T(8,128)(2,1)S(1)} %add_convert_fusion.3), channel_id=1, source_target_pairs={{0,24},{2,26},{4,28},{6,30},{8,16},{10,18},{12,20},{14,22},{16,8},... | collective-permute-start | bytes 1572872 | tf_op jit(solution)/shard_map/ppermute | solution.py:75
  200.9 44.0 %collective-permute-start.26 = (bf16[256,1024]{1,0:T(8,128)(2,1)S(1)}, bf16[256,1024]{1,0:T(8,128)(2,1)S(1)}, u32[]{:S(2)}, u32[]{:S(2)}) collective-permute-start(bf16[256,1024]{1,0:T(8,128)(2,1)S(1)} %add_convert_fusion.4), channel_id=1, source_target_pairs={{0,16},{2,18},{4,20},{6,22},{8,24},{10,26},{12,28},{14,30},{16,0},... | collective-permute-start | bytes 1572872 | tf_op jit(solution)/shard_map/ppermute | solution.py:75
  201.6 48.7 %dynamic-slice-start = ((f32[2048]{0:T(1024)}, s32[]{:T(128)}), f32[1024]{0:T(1024)S(1)}, s32[]{:S(2)}) async-start(f32[2048]{0:T(1024)} %param.25, s32[]{:T(128)} %select_n.249), calls=%async_computation | async-start | bytes 8704 | tf_op jit(solution)/shard_map/dynamic_slice | solution.py:70
  201.6 48.7 %dynamic-slice-start.1 = ((f32[2048]{0:T(1024)}, s32[]{:T(128)}), f32[1024]{0:T(1024)S(1)}, s32[]{:S(2)}) async-start(f32[2048]{0:T(1024)} %param.24, s32[]{:T(128)} %select_n.249), calls=%async_computation.1 | async-start | bytes 8704 | tf_op jit(solution)/shard_map/dynamic_slice | solution.py:70
  (4 other events, 3.8 us)
